TPU v7x, 768 devices: a whole 4x8x12 slice. The times are simulated.
768 devices in a mesh: fs: 24 (over z, core), tp: 32 (over y, x).
Axes of the slice: x: 4, y: 8, z: 12, core: 2. Of those that a mesh axis runs over, the one named last changes fastest.
Arguments:
- tokens: bfloat16 [4608, 2304], P('fs'), may hold values from -6 to 6
- gate_train: float32 [8, 2304, 2304], P(None, 'fs', 'tp'), may hold values from -0.125 to 0.125
- up_train: float32 [8, 2304, 2304], P(None, 'fs', 'tp'), may hold values from -0.125 to 0.125
- down_train: float32 [8, 2304, 2304], P(None, 'fs', 'tp'), may hold values from -0.125 to 0.125
- gain: float32 [2304], P('fs'), may hold values from 0.1 to 1.9
- routes: int32 [4608, 2], P('fs'), may hold values from 0 to 7, all different within a row; in each aligned block of 192 rows (0 to 191, 192 to 383, ...) at most 72 rows name the same one
- route_weights: float32 [4608, 2], P('fs'), may hold values from 0.1 to 1
Outputs:
- gate_new: bfloat16 [32, 576, 2304], P('tp')
- up_new: bfloat16 [32, 576, 2304], P('tp')
- down_new: bfloat16 [32, 576, 2304], P('tp')
- mixed: bfloat16 [4608, 2304], P('fs', 'tp')
Inputs may be any that keep to these rules, and one draw needn't show every extreme that they name: `routes`: each row names two different experts; in each aligned block of 192 rows at most 72 rows name one expert, a bound that some block reaches.
All inputs are finite; a program needn't handle non-finite values.
Results may differ from a plain program's by a relative error of at most 0.0095.
Values may be sent and summed in bfloat16 or wider, within the bound.
No kernel may reach another device: no remote copies, remote signals or barrier semaphores. Data moves between devices by JAX's collectives and lax.ppermute only.
A program may use at most 64 MiB of HBM per device.

v0:
```python
import jax
import jax.numpy as jnp
from jax import lax
from jax.sharding import PartitionSpec as P

CAP = 72


norm_eps = 1e-06


def sent_together(arrays, axis, split_dim, concat_dim, along):
    ends, at = ([], 0)
    for a in arrays[:-1]:
        at += a.shape[along]
        ends.append(at)
    both = jnp.concatenate(arrays, axis=along)
    return tuple(
        jnp.split(
            lax.all_to_all(both, axis, split_axis=split_dim, concat_axis=concat_dim, tiled=True),
            ends,
            axis=along,
        )
    )


def rows_first(arrays, axis, dims):
    turned = [jnp.moveaxis(a, dim, 0) for a, dim in zip(arrays, dims)]
    widths = [t[0].size for t in turned]
    both = jnp.concatenate([t.reshape(-1, w) for t, w in zip(turned, widths)], axis=1)
    out = lax.all_gather(both, axis, axis=0, tiled=True)
    pieces = jnp.split(out, [sum(widths[:k]) for k in range(1, len(widths))], axis=1)
    return tuple(
        (
            jnp.moveaxis(b.reshape(-1, *t.shape[1:]), 0, dim)
            for b, t, dim in zip(pieces, turned, dims)
        )
    )


def arrange(matrix, tp_count):
    experts, row_count, col_count = matrix.shape
    slices = tp_count // experts
    piece_width = col_count // slices
    shaped = matrix.reshape(experts, row_count, slices, piece_width)
    return shaped.transpose(0, 2, 3, 1).reshape(tp_count, piece_width, row_count)


def shards(tokens, gate_train, up_train, down_train, gain, routes, route_weights):
    tp_count = lax.axis_size("tp")
    experts = gate_train.shape[0]
    slices = tp_count // experts
    gain_column = gain[None, :, None]
    gate_round = (gate_train * gain_column).astype(jnp.bfloat16)
    up_round = (up_train * gain_column).astype(jnp.bfloat16)
    down_round = down_train.astype(jnp.bfloat16)
    moved = sent_together(
        (arrange(gate_round, tp_count), arrange(up_round, tp_count), arrange(down_round, tp_count)),
        "tp",
        0,
        1,
        2,
    )
    tokens_wide = tokens.astype(jnp.float32)
    normed = (
        tokens_wide
        * lax.rsqrt(jnp.mean(tokens_wide * tokens_wide, axis=1, keepdims=True) + norm_eps)
    ).astype(jnp.bfloat16)
    expert = lax.axis_index("tp") // slices
    matches = routes == expert
    member = jnp.any(matches, axis=1)
    slot_index = jnp.cumsum(member.astype(jnp.int32)) - 1
    marked = jnp.where(member, slot_index, -1)
    picker = (marked[None, :] == jnp.arange(CAP, dtype=jnp.int32)[:, None]).astype(jnp.bfloat16)
    chosen = jnp.dot(picker, normed, preferred_element_type=jnp.float32).astype(jnp.bfloat16)
    contract_last = (((1,), (1,)), ((), ()))
    gate_new, up_new, down_new = rows_first((moved[0], moved[1], moved[2]), "fs", (2, 2, 2))
    gate_pre = lax.dot_general(
        chosen, gate_new[0], contract_last, preferred_element_type=jnp.float32
    )
    up_pre = lax.dot_general(chosen, up_new[0], contract_last, preferred_element_type=jnp.float32)
    hidden = (jax.nn.silu(gate_pre) * up_pre).astype(jnp.bfloat16)
    partial_value = jnp.dot(hidden, down_new[0], preferred_element_type=jnp.float32).astype(
        jnp.bfloat16
    )
    labels = jnp.arange(experts, dtype=jnp.int32)
    member_all = jnp.any(routes[:, :, None] == labels[None, None, :], axis=1)
    slots_all = jnp.cumsum(member_all.astype(jnp.int32), axis=0) - 1
    slot_pair = jnp.take_along_axis(slots_all, routes, axis=1)
    flat_index = slot_pair * experts + routes
    received = lax.all_to_all(
        partial_value.reshape(CAP, tp_count, -1), "tp", split_axis=1, concat_axis=1, tiled=True
    )
    summed = jnp.sum(received.reshape(CAP, experts, slices, -1).astype(jnp.float32), axis=2)
    summed = summed.reshape(CAP * experts, -1)
    picked = jnp.take(summed, flat_index, axis=0)
    mixed = jnp.sum(route_weights[:, :, None] * picked, axis=1)
    return (gate_new, up_new, down_new, mixed.astype(jnp.bfloat16))


def solution(mesh):
    in_specs = (
        P("fs", None),
        P(None, "fs", "tp"),
        P(None, "fs", "tp"),
        P(None, "fs", "tp"),
        P("fs"),
        P("fs", None),
        P("fs", None),
    )
    out_specs = (P("tp", None, None), P("tp", None, None), P("tp", None, None), P("fs", "tp"))
    return jax.shard_map(shards, mesh=mesh, in_specs=in_specs, out_specs=out_specs, check_vma=False)
```

profile of v0, /device:TPU:1, one launch (start us, length us, event | category | flops | bytes accessed | tf_op | source)
XLA Modules:
  0.0 158.3 jit_solution(16805658789183874287)
XLA Ops:
  7.2 0.0 all-gather.2.cloned.1.call-start
  7.2 1.0 copy.156
  8.2 0.1 copy.134
  8.3 1.2 fusion.21
  9.5 0.1 copy.130
  9.6 0.1 copy.132
  9.6 0.2 pad_maximum_fusion
  9.9 0.0 copy-start.3
  9.9 0.2 copy.135
  10.1 25.2 %all_to_all.17 = bf16[32,18,288]{2,1,0:T(8,128)(2,1)S(1)} all-to-all(bf16[32,18,288]{2,1,0:T(8,128)(2,1)S(1)} %copy.135), channel_id=1, replica_groups=mesh['fs'=24,'tp'=32] {'tp'}, dimensions={0} | all-to-all | bytes 663552 | tf_op jit(solution)/shard_map/all_to_all | solution.py:20
  35.2 0.2 all_to_all.13
  35.4 0.1 slice_bitcast_fusion.5
  35.6 0.1 pad_maximum_fusion.1
  35.7 0.9 copy.136
  36.6 0.0 all-gather.2.cloned.1.call-update
  36.7 0.6 reduce-window.15
  37.3 0.2 slice_reduce_fusion
  37.6 0.1 copy.138
  37.7 0.1 reshape.138
  37.8 0.1 add_bitcast_fusion
  37.9 2.7 %gather_fusion.1 = s32[384]{0:T(512)S(1)} fusion(s32[192,8]{0,1:T(8,128)S(1)} %slice_add_fusion, s32[384]{0:T(512)S(1)} %reshape.138), kind=kCustom, calls=%fused_computation.1 | custom fusion | bytes 6144 | tf_op jit(solution)/shard_map/jit(take_along_axis)/gather | solution.py:89
  40.6 0.1 reshape.141
  40.8 0.1 copy.139
  40.9 0.3 reduce-window.19
  41.2 0.1 slice.22
  41.3 0.7 copy.140
  42.0 0.1 copy.143
  42.2 0.1 reshape.132
  42.3 0.8 copy.137
  43.1 0.1 slice_reduce_fusion.1
  43.2 0.3 fusion.8
  43.5 0.1 add_bitcast_fusion.1
  43.6 0.4 convolution_convert_fusion.1
  43.9 66.7 %all-gather.2.cloned.1.call-done = bf16[2304,1728]{1,0:T(8,128)(2,1)} async-done(((bf16[96,1728]{1,0:T(8,128)(2,1)}), bf16[2304,1728]{1,0:T(8,128)(2,1)}) %all-gather.2.cloned.1.call-update) | async-done | bytes 7962640 | tf_op jit(solution)/shard_map/all_gather | solution.py:31
  110.7 2.5 %fusion.3 = f32[72,576]{1,0:T(8,128)S(1)} fusion(bf16[72,2304]{1,0:T(8,128)(2,1)S(1)} %convolution_convert_fusion.1, bf16[2304,1728]{1,0:T(8,128)(2,1)} %all-gather.2.cloned.1.call-done), kind=kOutput, calls=%fused_computation.7 | convolution fusion | flops 191102976 | bytes 3446784 | tf_op jit(solution)/shard_map/dot_general | solution.py:78
  113.1 4.9 %convolution_convert_fusion = bf16[72,2304]{1,0:T(8,128)(2,1)S(1)} fusion(bf16[2304,1728]{1,0:T(8,128)(2,1)} %all-gather.2.cloned.1.call-done, bf16[72,2304]{1,0:T(8,128)(2,1)S(1)} %convolution_convert_fusion.1, f32[72,576]{1,0:T(8,128)S(1)} %fusion.3), kind=kOutput, calls=%fused_computation.2 | convolution fusion | flops 382620672 | bytes 6727680 | tf_op jit(solution)/shard_map/dot_general | solution.py:83
  118.1 1.3 reshape.125
  119.4 1.0 copy.141
  120.4 9.3 %all-to-all-start.1 = ((bf16[72,32,72]{2,0,1:T(8,128)(2,1)}), bf16[72,32,72]{2,0,1:T(8,128)(2,1)S(1)}, u32[]{:S(2)}, u32[]{:S(2)}) async-start(bf16[72,32,72]{2,0,1:T(8,128)(2,1)} %copy.141), calls=%async_computation.1 | async-start | bytes 1179648 | tf_op jit(solution)/shard_map/all_to_all | solution.py:91
  129.7 6.3 %slice_bitcast_fusion = (bf16[1,576,2304]{1,2,0:T(8,128)(2,1)}, bf16[1,576,2304]{1,2,0:T(8,128)(2,1)}, bf16[1,576,2304]{1,2,0:T(8,128)(2,1)S(1)}) fusion(bf16[2304,1728]{1,0:T(8,128)(2,1)} %all-gather.2.cloned.1.call-done), kind=kLoop, calls=%fused_computation.10 | loop fusion | bytes 15925248 | tf_op jit(solution)/shard_map/transpose | solution.py:35
  135.9 4.5 %copy.146 = bf16[1,576,2304]{2,1,0:T(8,128)(2,1)} copy(bf16[1,576,2304]{1,2,0:T(8,128)(2,1)} %get-tuple-element.22) | data formatting | bytes 5308416
  140.4 4.5 %copy.145 = bf16[1,576,2304]{2,1,0:T(8,128)(2,1)} copy(bf16[1,576,2304]{1,2,0:T(8,128)(2,1)} %get-tuple-element.23) | data formatting | bytes 5308416
  144.9 3.4 %copy.144 = bf16[1,576,2304]{2,1,0:T(8,128)(2,1)} copy(bf16[1,576,2304]{1,2,0:T(8,128)(2,1)S(1)} %get-tuple-element.24) | data formatting | bytes 5308416
  148.3 0.1 convert_reduce_fusion
  148.4 0.1 copy.157
  148.5 1.1 gather_fusion
  149.6 1.1 multiply_reduce_fusion
  150.7 0.7 copy.147
  (22 shorter events, 0.2 us)
Async XLA Ops:
  7.2 103.5 %all-gather.2.cloned.1.call-start = ((), (), s32[]{:S(2)}) async-start(), calls=%async_computation.2 | async-start | bytes 8601600 | tf_op jit(solution)/shard_map/all_gather | solution.py:31
  9.9 26.8 %copy-start.3 = (s32[192,2]{0,1:T(2,128)S(1)}, s32[192,2]{0,1:T(2,128)}, u32[]{:S(2)}) copy-start(s32[192,2]{0,1:T(2,128)} %param.12) | copy-start | bytes 4612
  37.9 4.4 %copy-start.4 = (f32[192,2]{0,1:T(2,128)S(1)}, f32[192,2]{0,1:T(2,128)}, u32[]{:S(2)}) copy-start(f32[192,2]{0,1:T(2,128)} %param.13) | copy-start | bytes 4612
  37.9 5.3 %copy-start = (bf16[192,2304]{1,0:T(8,128)(2,1)S(1)}, bf16[192,2304]{1,0:T(8,128)(2,1)}, u32[]{:S(2)}) copy-start(bf16[192,2304]{1,0:T(8,128)(2,1)} %param.7) | copy-start | bytes 2654212
  120.4 27.9 %all-to-all-start.1 = ((bf16[72,32,72]{2,0,1:T(8,128)(2,1)}), bf16[72,32,72]{2,0,1:T(8,128)(2,1)S(1)}, u32[]{:S(2)}, u32[]{:S(2)}) async-start(bf16[72,32,72]{2,0,1:T(8,128)(2,1)} %copy.141), calls=%async_computation.1 | async-start | bytes 1179648 | tf_op jit(solution)/shard_map/all_to_all | solution.py:91
  148.3 1.3 copy-start.1
  148.3 1.3 copy-start.2
Sparse Core Ops, SparseCore 0:
  36.8 73.8 all-gather.1
where the time goes:
time: 159 us; the launch traced here: 158 us
  waiting for transfers between devices  66.7 us (42%)
  local copies, waits for them, and re-layouts  30.8 us (19%)
  blocking collectives  25.2 us (16%)
  between operations  14.3 us (9%)
  starting transfers between devices  9.29 us (6%)
  matrix products  7.77 us (5%)
  other arithmetic  4.22 us (3%)
    all_gather x1, waiting for transfers between devices, rows_first(): out = lax.all_gather(both, axis, axis=0, tiled=True)  66.7 us
    all_to_all x1, blocking collectives, sent_together(): lax.all_to_all(both, axis, split_axis=split_dim, concat_axis=concat_dim,...  25.2 us
    unnamed x16, local copies, waits for them, and re-layouts  14.9 us
    all_to_all x1, starting transfers between devices, shards(): lax.all_to_all(partial_value.reshape(CAP, tp_count, -1), 'tp', split_axis...  9.25 us
    transpose x1, local copies, waits for them, and re-layouts, rows_first(): jnp.moveaxis(b.reshape(-1, *t.shape[1:]), 0, dim)  6.25 us
    dot_general x1, matrix products, shards(): jnp.dot(hidden, down_new[0], preferred_element_type=jnp.float32)  4.92 us
  transfers between devices with their start and end apart: 2, of which 1 were waited for; matrix products, arithmetic and copies ran while one was open for 16% of the time, Pallas kernels for 0%

commit v1 on v0

v1 whole, which is shorter than its diff:
```python
import jax
import jax.numpy as jnp
from jax import lax
from jax.experimental import pallas as pl
from jax.experimental.pallas import tpu as pltpu
from jax.sharding import PartitionSpec as P

CAP = 72
EPS = 1e-06
STEPS = (56, 28, 14, 8, 4, 2, 1)
LAST = (((1,), (1,)), ((), ()))


def arrange(matrix, tp_count):
    experts, rows, cols = matrix.shape
    slices = tp_count // experts
    turned = matrix.transpose(0, 2, 1)
    return turned.reshape(tp_count, cols // slices, rows)


def ranks(routes_t, experts):
    rows = routes_t.shape[1]
    labels = lax.broadcasted_iota(jnp.int32, (experts, rows), 0)
    first = routes_t[0:1, :] == labels
    second = routes_t[1:2, :] == labels
    member = jnp.where(first | second, 1.0, 0.0)
    before = lax.broadcasted_iota(jnp.int32, (rows, rows), 0) < lax.broadcasted_iota(
        jnp.int32, (rows, rows), 1
    )
    earlier = jnp.where(before, 1.0, 0.0).astype(jnp.bfloat16)
    rank = jnp.dot(member.astype(jnp.bfloat16), earlier, preferred_element_type=jnp.float32)
    return member, rank


def choose_kernel(expert_ref, tokens_ref, routes_ref, chosen_ref):
    wide = tokens_ref[...].astype(jnp.float32)
    scale = lax.rsqrt(jnp.mean(wide * wide, axis=1, keepdims=True) + EPS)
    normed = (wide * scale).astype(jnp.bfloat16)
    rows = wide.shape[0]
    member, rank = ranks(routes_ref[...], 8)
    own = lax.broadcasted_iota(jnp.int32, member.shape, 0) == expert_ref[0]
    marked = jnp.where(own & (member > 0.5), rank, -1.0)
    place = jnp.sum(jnp.where(own, marked, 0.0), axis=0, keepdims=True)
    slots = lax.broadcasted_iota(jnp.int32, (CAP, rows), 0).astype(jnp.float32)
    picker = jnp.where(slots == place, 1.0, 0.0).astype(jnp.bfloat16)
    chosen_ref[...] = jnp.dot(picker, normed, preferred_element_type=jnp.float32).astype(
        jnp.bfloat16
    )


def unpack(block_ref, start, out_ref):
    rows = out_ref.shape[0] // 4
    lanes = out_ref.shape[1]
    width = lanes // 4
    place = lax.broadcasted_iota(jnp.int32, (rows, lanes), 1)
    parts = [block_ref[s, start : start + rows, :] for s in range(4)]
    for g in range(4):
        merged = parts[(3 - g) % 4]
        for p in (2, 1, 0):
            merged = jnp.where(place < (p + 1) * width, parts[(p - g) % 4], merged)
        if g:
            merged = jnp.concatenate([merged[:, g * width :], merged[:, : g * width]], axis=1)
        out_ref[g * rows : (g + 1) * rows, :] = merged


def first_kernel(block_ref, chosen_ref, gate_ref, up_ref, hidden_ref, gate_sum, up_sum):
    step = pl.program_id(0)

    @pl.when(step == 0)
    def _():
        gate_sum[...] = jnp.zeros_like(gate_sum)
        up_sum[...] = jnp.zeros_like(up_sum)

    rows = gate_ref.shape[0] // 4
    unpack(block_ref, 0, gate_ref)
    unpack(block_ref, rows, up_ref)
    chosen = chosen_ref[...]
    gate_sum[...] += lax.dot_general(
        chosen, gate_ref[...], LAST, preferred_element_type=jnp.float32
    )
    up_sum[...] += lax.dot_general(chosen, up_ref[...], LAST, preferred_element_type=jnp.float32)

    @pl.when(step == pl.num_programs(0) - 1)
    def _():
        gate = gate_sum[...]
        hidden_ref[...] = (gate / (1.0 + jnp.exp(-gate)) * up_sum[...]).astype(jnp.bfloat16)


def second_kernel(block_ref, hidden_ref, down_ref, partial_ref):
    unpack(block_ref, 0, down_ref)
    product = jnp.dot(hidden_ref[...], down_ref[...], preferred_element_type=jnp.float32)
    partial_ref[...] = product.T.astype(jnp.bfloat16)


def combine_kernel(received_ref, routes_ref, weights_ref, mixed_ref):
    experts = 8
    slices = received_ref.shape[0] // experts
    routes = routes_ref[...]
    rows = routes.shape[1]
    _, rank = ranks(routes, experts)
    width = received_ref.shape[1]
    slots = lax.broadcasted_iota(jnp.int32, (CAP, rows), 0).astype(jnp.float32)
    totals = [jnp.zeros((width, rows), jnp.float32) for _ in range(2)]
    for e in range(experts):
        summed = received_ref[e * slices].astype(jnp.float32)
        for s in range(1, slices):
            summed = summed + received_ref[e * slices + s].astype(jnp.float32)
        high = summed.astype(jnp.bfloat16)
        low = (summed - high.astype(jnp.float32)).astype(jnp.bfloat16)
        at = slots == rank[e : e + 1, :]
        for j in range(2):
            named = routes[j : j + 1, :] == e
            pick = jnp.where(at & named, 1.0, 0.0).astype(jnp.bfloat16)
            totals[j] = (
                totals[j]
                + jnp.dot(high, pick, preferred_element_type=jnp.float32)
                + jnp.dot(low, pick, preferred_element_type=jnp.float32)
            )
    weights = weights_ref[...]
    mixed_ref[...] = (weights[0:1, :] * totals[0] + weights[1:2, :] * totals[1]).astype(
        jnp.bfloat16
    )


def shards(tokens, gate_train, up_train, down_train, gain, routes, route_weights):
    tp_count = lax.axis_size("tp")
    fs_count = lax.axis_size("fs")
    experts, features, _ = gate_train.shape
    slices = tp_count // experts
    gain_column = gain[None, :, None]
    gate_round = (gate_train * gain_column).astype(jnp.bfloat16)
    up_round = (up_train * gain_column).astype(jnp.bfloat16)
    down_round = down_train.astype(jnp.bfloat16)
    pieces = [arrange(a, tp_count) for a in (gate_round, up_round, down_round)]
    units = pieces[0].shape[1]
    moved = lax.all_to_all(
        jnp.concatenate(pieces, axis=1), "tp", split_axis=0, concat_axis=0, tiled=True
    )

    expert = (lax.axis_index("tp") // slices).astype(jnp.int32).reshape(1)
    routes_t = routes.T
    weights_t = route_weights.T
    rows, width = tokens.shape
    chosen = pl.pallas_call(
        choose_kernel,
        out_shape=jax.ShapeDtypeStruct((CAP, width), jnp.bfloat16),
        in_specs=[
            pl.BlockSpec(memory_space=pltpu.SMEM),
            pl.BlockSpec(memory_space=pltpu.VMEM),
            pl.BlockSpec(memory_space=pltpu.VMEM),
        ],
        out_specs=pl.BlockSpec(memory_space=pltpu.VMEM),
        cost_estimate=pl.CostEstimate(flops=2000000000, bytes_accessed=2000000, transcendentals=0),
    )(expert, tokens, routes_t)

    block_rows = tp_count * units
    quarter = block_rows // 4
    grouped = jnp.stack(
        [
            moved[:, m * units : (m + 1) * units].reshape(4, quarter, features)
            for m in range(3)
        ],
        axis=1,
    )
    shift = (4 - lax.axis_index("fs") % 4) % 4
    turned = lax.dynamic_slice_in_dim(jnp.concatenate([grouped, grouped], axis=0), shift, 4, 0)
    packed = jnp.concatenate([turned[p] for p in range(4)], axis=-1)
    lanes = 4 * features

    wide = packed.astype(jnp.float32)
    largest = jnp.max(jnp.abs(wide), axis=(1, 2))
    factor = jnp.ones_like(largest)
    power = jnp.zeros_like(largest)
    for b in STEPS:
        fits = largest * factor * 2.0**b <= 32768.0
        factor = jnp.where(fits, factor * 2.0**b, factor)
        power = jnp.where(fits, power + b, power)
    sent = (wide * factor[:, None, None]).astype(jnp.float16).reshape(3 * quarter, lanes)
    note = jnp.broadcast_to(power[:, None], (3, lanes // 3)).reshape(1, lanes)
    note = jnp.broadcast_to(note, (8, lanes)).astype(jnp.float16)
    gathered = lax.all_gather(jnp.concatenate([sent, note], axis=0), "fs", axis=0)
    left = jnp.stack(
        [gathered[:, 3 * quarter, m * (lanes // 3)] for m in range(3)], axis=1
    ).astype(jnp.float32)
    back = jnp.ones_like(left)
    for b in STEPS:
        holds = left >= b
        back = jnp.where(holds, back * 2.0**-b, back)
        left = jnp.where(holds, left - b, left)

    def returned(start, stop):
        part = gathered[:, start * quarter : stop * quarter].astype(jnp.float32)
        part = part.reshape(fs_count, stop - start, quarter, lanes)
        part = (part * back[:, start:stop, None, None]).astype(jnp.bfloat16)
        return part.reshape(fs_count, (stop - start) * quarter, lanes)

    both = returned(0, 2)
    third = returned(2, 3)
    steps = fs_count // 4
    matrix = jax.ShapeDtypeStruct((block_rows, width), jnp.bfloat16)
    matrix_spec = pl.BlockSpec((block_rows, lanes), lambda i: (0, i))
    gate_new, up_new, hidden = pl.pallas_call(
        first_kernel,
        grid=(steps,),
        out_shape=(matrix, matrix, jax.ShapeDtypeStruct((CAP, block_rows), jnp.bfloat16)),
        in_specs=[
            pl.BlockSpec((4, 2 * quarter, lanes), lambda i: (i, 0, 0)),
            pl.BlockSpec((CAP, lanes), lambda i: (0, i)),
        ],
        out_specs=(matrix_spec, matrix_spec, pl.BlockSpec((CAP, block_rows), lambda i: (0, 0))),
        scratch_shapes=[pltpu.VMEM((CAP, block_rows), jnp.float32)] * 2,
    )(both, chosen)
    down_new, partial = pl.pallas_call(
        second_kernel,
        grid=(steps,),
        out_shape=(matrix, jax.ShapeDtypeStruct((width, CAP), jnp.bfloat16)),
        in_specs=[
            pl.BlockSpec((4, quarter, lanes), lambda i: (i, 0, 0)),
            pl.BlockSpec((CAP, block_rows), lambda i: (0, 0)),
        ],
        out_specs=(matrix_spec, pl.BlockSpec((lanes, CAP), lambda i: (i, 0))),
    )(third, hidden)

    received = lax.all_to_all(
        partial.reshape(tp_count, width // tp_count, CAP),
        "tp",
        split_axis=0,
        concat_axis=0,
        tiled=True,
    )
    mixed = pl.pallas_call(
        combine_kernel,
        out_shape=jax.ShapeDtypeStruct((width // tp_count, rows), jnp.bfloat16),
    )(received, routes_t, weights_t)
    return (gate_new[None], up_new[None], down_new[None], mixed.T)


def solution(mesh):
    in_specs = (
        P("fs", None),
        P(None, "fs", "tp"),
        P(None, "fs", "tp"),
        P(None, "fs", "tp"),
        P("fs"),
        P("fs", None),
        P("fs", None),
    )
    out_specs = (P("tp", None, None), P("tp", None, None), P("tp", None, None), P("fs", "tp"))
    return jax.shard_map(shards, mesh=mesh, in_specs=in_specs, out_specs=out_specs, check_vma=False)
```

time: 159 us -> 149 us (0.937)
  blocking collectives: 25.2 us -> 91.5 us
  waiting for transfers between devices: 66.7 us -> 9.78 us
  local copies, waits for them, and re-layouts: 30.8 us -> 4.22 us
  Pallas kernels: 0 us -> 18 us
  between operations: 14.3 us -> 0.8 us
  other arithmetic: 4.22 us -> 13 us
  matrix products: 7.77 us -> 0 us
    all_gather x0 -> x1, blocking collectives: none -> 68.9 us  [shards(): lax.all_gather(jnp.concatenate([sent, note], axis=0), 'fs', axis=0)]
    all_gather x1 -> x0, waiting for transfers between devices: 66.7 us -> none  [rows_first(): out = lax.all_gather(both, axis, axis=0, tiled=True)]
    pallas_call x0 -> x4, Pallas kernels: none -> 18 us  [the longest x1 7.49 us: shards(): pl.pallas_call(first_kernel, grid=(steps,), out_shape=(matrix, matrix, ja...]
    unnamed x16 -> x2, local copies, waits for them, and re-layouts: 14.9 us -> 2.82 us
    all_to_all x1, waiting for transfers between devices: 0.01 us -> 9.78 us  [shards(): lax.all_to_all(jnp.concatenate(pieces, axis=1), 'tp', split_axis=0, conca...]
    convert_element_type x1 -> x4, other arithmetic: 1.19 us -> 9.1 us  [the longest x2 8.78 us: returned(): part = (part * back[:, start:stop, None, None]).astype(jnp.bfloat16)]
    dot_general x3 -> x0, matrix products: 7.77 us -> none  [the longest x1 4.92 us: shards(): jnp.dot(hidden, down_new[0], preferred_element_type=jnp.float32)]
    transpose x4 -> x0, local copies, waits for them, and re-layouts: 6.43 us -> none  [the longest x1 6.25 us: rows_first(): jnp.moveaxis(b.reshape(-1, *t.shape[1:]), 0, dim)]
  transfers between devices with their start and end apart: 2 -> 1, of which waited for: 1 -> 1; matrix products, arithmetic and copies ran while one was open for 16% -> 0% of each run, Pallas kernels for 0% -> 2%
where the time goes in v1:
time: 149 us; the launch traced here: 148 us
  blocking collectives  91.5 us (61%)
  Pallas kernels  18 us (12%)
  other arithmetic  13 us (9%)
  starting transfers between devices  10.5 us (7%)
  waiting for transfers between devices  9.78 us (7%)
  local copies, waits for them, and re-layouts  4.22 us (3%)
    all_gather x1, blocking collectives, shards(): lax.all_gather(jnp.concatenate([sent, note], axis=0), 'fs', axis=0)  68.9 us
    all_to_all x1, blocking collectives, shards(): lax.all_to_all(partial.reshape(tp_count, width // tp_count, CAP), 'tp', s...  22.6 us
    all_to_all x1, starting transfers between devices, shards(): lax.all_to_all(jnp.concatenate(pieces, axis=1), 'tp', split_axis=0, conca...  10.5 us
    all_to_all x1, waiting for transfers between devices, shards(): lax.all_to_all(jnp.concatenate(pieces, axis=1), 'tp', split_axis=0, conca...  9.78 us
    convert_element_type x2, other arithmetic, returned(): part = (part * back[:, start:stop, None, None]).astype(jnp.bfloat16)  8.78 us
    pallas_call x1, Pallas kernels, shards(): pl.pallas_call(first_kernel, grid=(steps,), out_shape=(matrix, matrix, ja...  7.49 us
    pallas_call x1, Pallas kernels, shards(): pl.pallas_call(second_kernel, grid=(steps,), out_shape=(matrix, jax.Shape...  5.79 us
  transfers between devices with their start and end apart: 1, of which 1 were waited for; matrix products, arithmetic and copies ran while one was open for 0% of the time, Pallas kernels for 2%

profile of v1, /device:TPU:1, one launch (start us, length us, event | category | flops | bytes accessed | tf_op | source)
XLA Modules:
  0.0 147.8 jit_solution(4069110916159027353)
XLA Ops:
  0.6 1.1 fusion.5
  1.8 0.1 reshape.130
  1.8 0.1 reshape.131
  1.9 1.0 convert_bitcast_fusion
  2.9 0.1 reshape.132
  2.9 1.0 pad_maximum_fusion
  3.9 10.5 %all-to-all-start = ((bf16[32,54,96]{2,1,0:T(8,128)(2,1)}), bf16[32,54,96]{2,1,0:T(8,128)(2,1)S(1)}, u32[]{:S(2)}, u32[]{:S(2)}) async-start(bf16[32,54,96]{2,1,0:T(8,128)(2,1)} %pad_maximum_fusion), calls=%async_computation | async-start | bytes 917504 | tf_op jit(solution)/shard_map/all_to_all | solution.py:136
  14.4 2.4 %shard_map.102.chosen_ref = bf16[72,2304]{1,0:T(8,128)(2,1)} custom-call(s32[1]{0:T(128)} %bitcast.13.expert_ref, bf16[192,2304]{1,0:T(8,128)(2,1)} %tokens_ref.1, s32[2,192]{1,0:T(2,128)} %bitcast.52), custom_call_target="tpu_custom_call" | custom-call | flops 2000000000 | bytes 2000000 | tf_op jit(solution)/shard_map/pallas_call | solution.py:144
  16.8 9.8 %all-to-all-done = bf16[32,54,96]{2,1,0:T(8,128)(2,1)S(1)} async-done(((bf16[32,54,96]{2,1,0:T(8,128)(2,1)}), bf16[32,54,96]{2,1,0:T(8,128)(2,1)S(1)}, u32[]{:S(2)}, u32[]{:S(2)}) %all-to-all-start) | async-done | bytes 331808 | tf_op jit(solution)/shard_map/all_to_all | solution.py:136
  26.6 0.1 fusion.10
  26.8 0.1 stack_reshape.10
  26.8 0.1 stack_reshape.11
  26.9 0.1 stack_reshape.9
  27.0 0.4 fusion.2
  27.4 0.1 fusion.11
  27.5 0.3 abs_reduce_fusion
  27.8 0.1 mul.317
  27.9 0.1 mul.318
  28.0 0.1 broadcast_bitcast_fusion
  28.1 0.3 multiply_convert_fusion.2
  28.4 0.1 pad_maximum_fusion.1
  28.5 68.9 %all-gather.2 = f16[10560,384]{1,0:T(8,128)(2,1)S(1)} all-gather(f16[440,384]{1,0:T(8,128)(2,1)S(1)} %pad_maximum_fusion.1), channel_id=2, replica_groups=mesh['fs'=24,'tp'=32] {'fs'}, dimensions={0}, use_global_device_ids=true | all-gather | bytes 8448000 | tf_op jit(solution)/shard_map/all_gather | solution.py:181
  97.4 0.0 copy-start
  97.4 0.3 slice_reduce_fusion.2
  97.7 2.8 %copy-done = f16[10560,384]{1,0:T(8,128)(2,1)} copy-done((f16[10560,384]{1,0:T(8,128)(2,1)}, f16[10560,384]{1,0:T(8,128)(2,1)S(1)}, u32[]{:S(2)}) %copy-start) | copy-done | bytes 8110104
  100.5 2.4 %multiply_convert_fusion.1.block_ref = bf16[24,144,384]{2,1,0:T(8,128)(2,1)} fusion(f16[24,440,384]{2,1,0:T(8,128)(2,1)S(1)} %bitcast.44, f32[24]{0:T(128)S(1)} %slice_bitcast_fusion), kind=kLoop, calls=%fused_computation.1 | loop fusion | flops 3981312 | bytes 5308512 | tf_op jit(solution)/shard_map/convert_element_type | solution.py:194
  103.0 0.1 copy.18
  103.0 0.1 mul.334
  103.1 0.1 mul.335
  103.2 6.4 %multiply_convert_fusion.block_ref = bf16[24,288,384]{2,1,0:T(8,128)(2,1)} fusion(f16[24,440,384]{2,1,0:T(8,128)(2,1)} %bitcast.45, f32[24,288]{1,0:T(8,128)S(1)} %mul.335), kind=kLoop, calls=%fused_computation | loop fusion | flops 7962624 | bytes 10644480 | tf_op jit(solution)/shard_map/convert_element_type | solution.py:194
  109.6 7.5 %shard_map.103 = (bf16[576,2304]{1,0:T(8,128)(2,1)}, bf16[576,2304]{1,0:T(8,128)(2,1)}, bf16[72,576]{1,0:T(8,128)(2,1)}) custom-call(bf16[24,288,384]{2,1,0:T(8,128)(2,1)} %multiply_convert_fusion.block_ref, bf16[72,2304]{1,0:T(8,128)(2,1)} %shard_map.102.chosen_ref), custom_call_target="tpu_custom_call" | custom-call | tf_op jit(solution)/shard_map/pallas_call | solution.py:202
  117.1 5.8 %shard_map.104 = (bf16[576,2304]{1,0:T(8,128)(2,1)}, bf16[2304,72]{1,0:T(8,128)(2,1)}) custom-call(bf16[24,144,384]{2,1,0:T(8,128)(2,1)} %multiply_convert_fusion.1.block_ref, bf16[72,576]{1,0:T(8,128)(2,1)} %get-tuple-element.11.hidden_ref), custom_call_target="tpu_custom_call" | custom-call | tf_op jit(solution)/shard_map/pallas_call | solution.py:213
  122.9 22.6 %all_to_all.10.received_ref = bf16[32,72,72]{2,1,0:T(8,128)(2,1)} all-to-all(bf16[32,72,72]{2,1,0:T(8,128)(2,1)} %bitcast.46), channel_id=1, replica_groups=mesh['fs'=24,'tp'=32] {'tp'}, dimensions={0} | all-to-all | bytes 663552 | tf_op jit(solution)/shard_map/all_to_all | solution.py:224
  145.5 2.4 %shard_map.105 = bf16[72,192]{1,0:T(8,128)(2,1)} custom-call(bf16[32,72,72]{2,1,0:T(8,128)(2,1)} %all_to_all.10.received_ref, s32[2,192]{1,0:T(2,128)} %bitcast.53, f32[2,192]{1,0:T(2,128)} %bitcast.54), custom_call_target="tpu_custom_call" | custom-call | tf_op jit(solution)/shard_map/pallas_call | solution.py:231
  (6 shorter events, 0.1 us)
Async XLA Ops:
  3.9 22.7 %all-to-all-start = ((bf16[32,54,96]{2,1,0:T(8,128)(2,1)}), bf16[32,54,96]{2,1,0:T(8,128)(2,1)S(1)}, u32[]{:S(2)}, u32[]{:S(2)}) async-start(bf16[32,54,96]{2,1,0:T(8,128)(2,1)} %pad_maximum_fusion), calls=%async_computation | async-start | bytes 917504 | tf_op jit(solution)/shard_map/all_to_all | solution.py:136
  97.4 3.1 %copy-start = (f16[10560,384]{1,0:T(8,128)(2,1)}, f16[10560,384]{1,0:T(8,128)(2,1)S(1)}, u32[]{:S(2)}) copy-start(f16[10560,384]{1,0:T(8,128)(2,1)S(1)} %all-gather.2) | copy-start | bytes 24330244

commit v2 on v1

--- a/solution.py
+++ b/solution.py
@@ -63,33 +63,55 @@
         out_ref[g * rows : (g + 1) * rows, :] = merged
 
 
-def first_kernel(block_ref, chosen_ref, gate_ref, up_ref, hidden_ref, gate_sum, up_sum):
-    step = pl.program_id(0)
-
-    @pl.when(step == 0)
+def product_kernel(
+    both_ref,
+    third_ref,
+    chosen_ref,
+    gate_ref,
+    up_ref,
+    partial_ref,
+    down_ref,
+    hidden_ref,
+    gate_sum,
+    up_sum,
+):
+    i = pl.program_id(0)
+    steps = both_ref.shape[0] // 4
+    lanes = gate_ref.shape[1]
+    rows = gate_ref.shape[0] // 4
+
+    @pl.when(i < steps)
     def _():
-        gate_sum[...] = jnp.zeros_like(gate_sum)
-        up_sum[...] = jnp.zeros_like(up_sum)
-
-    rows = gate_ref.shape[0] // 4
-    unpack(block_ref, 0, gate_ref)
-    unpack(block_ref, rows, up_ref)
-    chosen = chosen_ref[...]
-    gate_sum[...] += lax.dot_general(
-        chosen, gate_ref[...], LAST, preferred_element_type=jnp.float32
-    )
-    up_sum[...] += lax.dot_general(chosen, up_ref[...], LAST, preferred_element_type=jnp.float32)
-
-    @pl.when(step == pl.num_programs(0) - 1)
+        unpack(both_ref.at[pl.ds(4 * i, 4)], 0, gate_ref)
+        unpack(both_ref.at[pl.ds(4 * i, 4)], rows, up_ref)
+        chosen = chosen_ref[:, pl.ds(pl.multiple_of(i * lanes, 128), lanes)]
+        gate = lax.dot_general(chosen, gate_ref[...], LAST, preferred_element_type=jnp.float32)
+        up = lax.dot_general(chosen, up_ref[...], LAST, preferred_element_type=jnp.float32)
+
+        @pl.when(i == 0)
+        def _():
+            gate_sum[...] = gate
+            up_sum[...] = up
+
+        @pl.when(i > 0)
+        def _():
+            gate_sum[...] += gate
+            up_sum[...] += up
+
+    @pl.when(i == steps - 1)
     def _():
-        gate = gate_sum[...]
-        hidden_ref[...] = (gate / (1.0 + jnp.exp(-gate)) * up_sum[...]).astype(jnp.bfloat16)
-
-
-def second_kernel(block_ref, hidden_ref, down_ref, partial_ref):
-    unpack(block_ref, 0, down_ref)
-    product = jnp.dot(hidden_ref[...], down_ref[...], preferred_element_type=jnp.float32)
-    partial_ref[...] = product.T.astype(jnp.bfloat16)
+        total = gate_sum[...]
+        hidden_ref[...] = (total / (1.0 + jnp.exp(-total)) * up_sum[...]).astype(jnp.bfloat16)
+
+    @pl.when(i >= steps)
+    def _():
+        unpack(third_ref.at[pl.ds(4 * (i - steps), 4)], 0, down_ref)
+        product = jnp.dot(hidden_ref[...], down_ref[...], preferred_element_type=jnp.float32)
+        partial_ref[...] = product.T.astype(jnp.bfloat16)
+
+
+def output_kernel(third_ref, down_ref):
+    unpack(third_ref.at[pl.ds(4 * pl.program_id(0), 4)], 0, down_ref)
 
 
 def combine_kernel(received_ref, routes_ref, weights_ref, mixed_ref):
@@ -151,6 +173,7 @@
         ],
         out_specs=pl.BlockSpec(memory_space=pltpu.VMEM),
         cost_estimate=pl.CostEstimate(flops=2000000000, bytes_accessed=2000000, transcendentals=0),
+        compiler_params=pltpu.CompilerParams(vmem_limit_bytes=24 * 2**20),
     )(expert, tokens, routes_t)
 
     block_rows = tp_count * units
@@ -197,29 +220,41 @@
     both = returned(0, 2)
     third = returned(2, 3)
     steps = fs_count // 4
+    whole = pl.BlockSpec(memory_space=pltpu.VMEM)
     matrix = jax.ShapeDtypeStruct((block_rows, width), jnp.bfloat16)
-    matrix_spec = pl.BlockSpec((block_rows, lanes), lambda i: (0, i))
-    gate_new, up_new, hidden = pl.pallas_call(
-        first_kernel,
+    held = pl.BlockSpec((block_rows, lanes), lambda i: (0, jnp.minimum(i, steps - 1)))
+    gate_new, up_new, partial = pl.pallas_call(
+        product_kernel,
+        grid=(2 * steps,),
+        out_shape=(matrix, matrix, jax.ShapeDtypeStruct((width, CAP), jnp.bfloat16)),
+        in_specs=[whole] * 3,
+        out_specs=(
+            held,
+            held,
+            pl.BlockSpec((lanes, CAP), lambda i: (jnp.maximum(i - steps, 0), 0)),
+        ),
+        scratch_shapes=[
+            pltpu.VMEM((block_rows, lanes), jnp.bfloat16),
+            pltpu.VMEM((CAP, block_rows), jnp.bfloat16),
+            pltpu.VMEM((CAP, block_rows), jnp.float32),
+            pltpu.VMEM((CAP, block_rows), jnp.float32),
+        ],
+        compiler_params=pltpu.CompilerParams(vmem_limit_bytes=24 * 2**20),
+        cost_estimate=pl.CostEstimate(
+            flops=3 * 2 * CAP * block_rows * width, bytes_accessed=2**23, transcendentals=0
+        ),
+    )(both, third, chosen)
+    down_new = pl.pallas_call(
+        output_kernel,
         grid=(steps,),
-        out_shape=(matrix, matrix, jax.ShapeDtypeStruct((CAP, block_rows), jnp.bfloat16)),
-        in_specs=[
-            pl.BlockSpec((4, 2 * quarter, lanes), lambda i: (i, 0, 0)),
-            pl.BlockSpec((CAP, lanes), lambda i: (0, i)),
-        ],
-        out_specs=(matrix_spec, matrix_spec, pl.BlockSpec((CAP, block_rows), lambda i: (0, 0))),
-        scratch_shapes=[pltpu.VMEM((CAP, block_rows), jnp.float32)] * 2,
-    )(both, chosen)
-    down_new, partial = pl.pallas_call(
-        second_kernel,
-        grid=(steps,),
-        out_shape=(matrix, jax.ShapeDtypeStruct((width, CAP), jnp.bfloat16)),
-        in_specs=[
-            pl.BlockSpec((4, quarter, lanes), lambda i: (i, 0, 0)),
-            pl.BlockSpec((CAP, block_rows), lambda i: (0, 0)),
-        ],
-        out_specs=(matrix_spec, pl.BlockSpec((lanes, CAP), lambda i: (i, 0))),
-    )(third, hidden)
+        out_shape=matrix,
+        in_specs=[whole],
+        out_specs=pl.BlockSpec((block_rows, lanes), lambda i: (0, i)),
+        compiler_params=pltpu.CompilerParams(vmem_limit_bytes=24 * 2**20),
+        cost_estimate=pl.CostEstimate(
+            flops=5000000000, bytes_accessed=2**24, transcendentals=0
+        ),
+    )(third)
 
     received = lax.all_to_all(
         partial.reshape(tp_count, width // tp_count, CAP),
@@ -231,6 +266,7 @@
     mixed = pl.pallas_call(
         combine_kernel,
         out_shape=jax.ShapeDtypeStruct((width // tp_count, rows), jnp.bfloat16),
+        compiler_params=pltpu.CompilerParams(vmem_limit_bytes=24 * 2**20),
     )(received, routes_t, weights_t)
     return (gate_new[None], up_new[None], down_new[None], mixed.T)
 

time: 149 us -> 140 us (0.940)
  blocking collectives: 91.5 us -> 70.3 us
  waiting for transfers between devices: 9.78 us -> 24.6 us
  Pallas kernels: 18 us -> 12.9 us
  starting transfers between devices: 10.5 us -> 14.7 us
  other arithmetic: 13 us -> 10.7 us
    all_to_all x1 -> x0, blocking collectives: 22.6 us -> none  [shards(): lax.all_to_all(partial.reshape(tp_count, width // tp_count, CAP), 'tp', s...]
    all_to_all x0 -> x1, waiting for transfers between devices: none -> 14.8 us  [shards(): lax.all_to_all(partial.reshape(tp_count, width // tp_count, CAP), 'tp', s...]
    all_to_all x0 -> x1, starting transfers between devices: none -> 4.2 us  [shards(): lax.all_to_all(partial.reshape(tp_count, width // tp_count, CAP), 'tp', s...]
    convert_element_type x2, other arithmetic: 8.78 us -> 6.49 us  [returned(): part = (part * back[:, start:stop, None, None]).astype(jnp.bfloat16)]
    pallas_call x2, Pallas kernels: 13.3 us -> 11.1 us  [the longest x1 8.1 us: shards(): pl.pallas_call(product_kernel, grid=(2 * steps,), out_shape=(matrix, matr...]
    pallas_call x1, Pallas kernels: 2.42 us -> 0.54 us  [shards(): pl.pallas_call(choose_kernel, out_shape=jax.ShapeDtypeStruct((CAP, width)...]
  transfers between devices with their start and end apart: 1 -> 2, of which waited for: 1 -> 2; matrix products, arithmetic and copies ran while one was open for 0% -> 0% of each run, Pallas kernels for 2% -> 3%
where the time goes in v2:
time: 140 us; the launch traced here: 139 us
  blocking collectives  70.3 us (50%)
  waiting for transfers between devices  24.6 us (18%)
  starting transfers between devices  14.7 us (10%)
  Pallas kernels  12.9 us (9%)
  other arithmetic  10.7 us (8%)
  local copies, waits for them, and re-layouts  4.92 us (4%)
    all_gather x1, blocking collectives, shards(): lax.all_gather(jnp.concatenate([sent, note], axis=0), 'fs', axis=0)  70.3 us
    all_to_all x1, waiting for transfers between devices, shards(): lax.all_to_all(partial.reshape(tp_count, width // tp_count, CAP), 'tp', s...  14.8 us
    all_to_all x1, starting transfers between devices, shards(): lax.all_to_all(jnp.concatenate(pieces, axis=1), 'tp', split_axis=0, conca...  10.5 us
    all_to_all x1, waiting for transfers between devices, shards(): lax.all_to_all(jnp.concatenate(pieces, axis=1), 'tp', split_axis=0, conca...  9.8 us
    pallas_call x1, Pallas kernels, shards(): pl.pallas_call(product_kernel, grid=(2 * steps,), out_shape=(matrix, matr...  8.1 us
    convert_element_type x2, other arithmetic, returned(): part = (part * back[:, start:stop, None, None]).astype(jnp.bfloat16)  6.49 us
    all_to_all x1, starting transfers between devices, shards(): lax.all_to_all(partial.reshape(tp_count, width // tp_count, CAP), 'tp', s...  4.2 us
    pallas_call x1, Pallas kernels, shards(): pl.pallas_call(output_kernel, grid=(steps,), out_shape=matrix, in_specs=[...  3.02 us
  transfers between devices with their start and end apart: 2, of which 2 were waited for; matrix products, arithmetic and copies ran while one was open for 0% of the time, Pallas kernels for 3%

profile of v2, /device:TPU:1, one launch (start us, length us, event | category | flops | bytes accessed | tf_op | source)
XLA Modules:
  0.0 139.0 jit_solution(11820252766398237250)
XLA Ops:
  0.6 1.0 convert_bitcast_fusion
  1.6 0.1 reshape.132
  1.7 1.1 fusion.5
  2.8 0.1 reshape.131
  2.9 0.1 reshape.130
  2.9 1.0 pad_maximum_fusion
  3.9 10.5 %all-to-all-start = ((bf16[32,54,96]{2,1,0:T(8,128)(2,1)}), bf16[32,54,96]{2,1,0:T(8,128)(2,1)S(1)}, u32[]{:S(2)}, u32[]{:S(2)}) async-start(bf16[32,54,96]{2,1,0:T(8,128)(2,1)} %pad_maximum_fusion), calls=%async_computation | async-start | bytes 917504 | tf_op jit(solution)/shard_map/all_to_all | solution.py:158
  14.4 0.0 copy-start.1
  14.4 0.7 copy-done.1
  15.1 0.0 copy-start.4
  15.1 1.2 copy-done.4
  16.3 0.5 shard_map.102.chosen_ref
  16.8 9.8 %all-to-all-done = bf16[32,54,96]{2,1,0:T(8,128)(2,1)S(1)} async-done(((bf16[32,54,96]{2,1,0:T(8,128)(2,1)}), bf16[32,54,96]{2,1,0:T(8,128)(2,1)S(1)}, u32[]{:S(2)}, u32[]{:S(2)}) %all-to-all-start) | async-done | bytes 331808 | tf_op jit(solution)/shard_map/all_to_all | solution.py:158
  26.6 0.1 fusion.10
  26.8 0.1 stack_reshape.9
  26.8 0.1 stack_reshape.10
  26.9 0.1 stack_reshape.11
  27.0 0.4 fusion.2
  27.4 0.1 fusion.11
  27.5 0.3 abs_reduce_fusion
  27.9 0.1 broadcast_bitcast_fusion
  27.9 0.1 mul.317
  28.0 0.1 mul.318
  28.1 0.3 multiply_convert_fusion.2
  28.4 0.1 pad_maximum_fusion.1
  28.5 70.3 %all-gather.2 = f16[10560,384]{1,0:T(8,128)(2,1)} all-gather(f16[440,384]{1,0:T(8,128)(2,1)S(1)} %pad_maximum_fusion.1), channel_id=2, replica_groups=mesh['fs'=24,'tp'=32] {'fs'}, dimensions={0}, use_global_device_ids=true | all-gather | bytes 8448000 | tf_op jit(solution)/shard_map/all_gather | solution.py:204
  98.8 1.1 slice_reduce_fusion.2
  99.9 0.1 copy.18
  100.0 0.1 mul.334
  100.1 0.1 mul.335
  100.2 3.8 %multiply_convert_fusion.both_ref = bf16[24,288,384]{2,1,0:T(8,128)(2,1)S(1)} fusion(f16[24,440,384]{2,1,0:T(8,128)(2,1)} %bitcast.12, f32[24,288]{1,0:T(8,128)S(1)} %mul.335), kind=kLoop, calls=%fused_computation | loop fusion | flops 7962624 | bytes 10644480 | tf_op jit(solution)/shard_map/convert_element_type | solution.py:217
  104.0 2.7 %multiply_convert_fusion.1.third_ref = bf16[24,144,384]{2,1,0:T(8,128)(2,1)S(1)} fusion(f16[24,440,384]{2,1,0:T(8,128)(2,1)} %bitcast.12, f32[24]{0:T(128)S(1)} %slice_bitcast_fusion), kind=kLoop, calls=%fused_computation.1 | loop fusion | flops 3981312 | bytes 5308512 | tf_op jit(solution)/shard_map/convert_element_type | solution.py:217
  106.7 8.1 %shard_map.103 = (bf16[576,2304]{1,0:T(8,128)(2,1)}, bf16[576,2304]{1,0:T(8,128)(2,1)}, bf16[2304,72]{1,0:T(8,128)(2,1)S(1)}) custom-call(bf16[24,288,384]{2,1,0:T(8,128)(2,1)S(1)} %multiply_convert_fusion.both_ref, bf16[24,144,384]{2,1,0:T(8,128)(2,1)S(1)} %multiply_convert_fusion.1.third_ref, bf16[72,2304]{1,0:T(8,128)(2,1)S(1)} %shard_map.102.chosen_ref), custom_call_target="tpu_custom_call" | custom-call | flops 573308928 | bytes 8388608 | tf_op jit(solution)/shard_map/pallas_call | solution.py:226
  114.8 0.0 copy-start
  114.8 0.8 copy-done
  115.6 4.2 %all-to-all-start.1 = ((bf16[32,72,72]{2,1,0:T(8,128)(2,1)}), bf16[32,72,72]{2,1,0:T(8,128)(2,1)S(1)}, u32[]{:S(2)}, u32[]{:S(2)}) async-start(bf16[32,72,72]{2,1,0:T(8,128)(2,1)} %bitcast.43), calls=%async_computation.1 | async-start | bytes 1179648 | tf_op jit(solution)/shard_map/all_to_all | solution.py:259
  119.9 0.0 copy-start.2
  119.9 0.0 copy-start.3
  119.9 3.0 %shard_map.104 = bf16[576,2304]{1,0:T(8,128)(2,1)} custom-call(bf16[24,144,384]{2,1,0:T(8,128)(2,1)S(1)} %multiply_convert_fusion.1.third_ref), custom_call_target="tpu_custom_call" | custom-call | flops 5000000000 | bytes 16777216 | tf_op jit(solution)/shard_map/pallas_call | solution.py:247
  122.9 14.8 %all-to-all-done.1.received_ref = bf16[32,72,72]{2,1,0:T(8,128)(2,1)S(1)} async-done(((bf16[32,72,72]{2,1,0:T(8,128)(2,1)}), bf16[32,72,72]{2,1,0:T(8,128)(2,1)S(1)}, u32[]{:S(2)}, u32[]{:S(2)}) %all-to-all-start.1) | async-done | bytes 331808 | tf_op jit(solution)/shard_map/all_to_all | solution.py:259
  137.7 0.0 copy-done.2
  137.7 0.0 copy-done.3
  137.7 1.3 shard_map.105
  (6 shorter events, 0.1 us)
Async XLA Ops:
  3.9 22.7 %all-to-all-start = ((bf16[32,54,96]{2,1,0:T(8,128)(2,1)}), bf16[32,54,96]{2,1,0:T(8,128)(2,1)S(1)}, u32[]{:S(2)}, u32[]{:S(2)}) async-start(bf16[32,54,96]{2,1,0:T(8,128)(2,1)} %pad_maximum_fusion), calls=%async_computation | async-start | bytes 917504 | tf_op jit(solution)/shard_map/all_to_all | solution.py:158
  14.4 0.7 copy-start.1
  15.1 1.2 copy-start.4
  114.8 0.8 copy-start
  115.6 22.1 %all-to-all-start.1 = ((bf16[32,72,72]{2,1,0:T(8,128)(2,1)}), bf16[32,72,72]{2,1,0:T(8,128)(2,1)S(1)}, u32[]{:S(2)}, u32[]{:S(2)}) async-start(bf16[32,72,72]{2,1,0:T(8,128)(2,1)} %bitcast.43), calls=%async_computation.1 | async-start | bytes 1179648 | tf_op jit(solution)/shard_map/all_to_all | solution.py:259
  119.9 17.9 %copy-start.2 = (s32[192,2]{0,1:T(2,128)S(1)}, s32[192,2]{0,1:T(2,128)}, u32[]{:S(2)}) copy-start(s32[192,2]{0,1:T(2,128)} %param.12) | copy-start | bytes 4612
  119.9 17.8 %copy-start.3 = (f32[192,2]{0,1:T(2,128)S(1)}, f32[192,2]{0,1:T(2,128)}, u32[]{:S(2)}) copy-start(f32[192,2]{0,1:T(2,128)} %param.13) | copy-start | bytes 4612

commit v3 on v2

--- a/solution.py
+++ b/solution.py
@@ -48,42 +48,55 @@
     )
 
 
-def unpack(block_ref, start, out_ref):
+def by_lane(parts, shift):
+    lanes = parts[0].shape[1]
+    place = lax.broadcasted_iota(jnp.int32, parts[0].shape, 1)
+    merged = parts[(3 - shift) % 4]
+    for p in (2, 1, 0):
+        merged = jnp.where(place < (p + 1) * (lanes // 4), parts[(p - shift) % 4], merged)
+    return merged
+
+
+def unpack(block_ref, matrix, out_ref):
     rows = out_ref.shape[0] // 4
     lanes = out_ref.shape[1]
     width = lanes // 4
-    place = lax.broadcasted_iota(jnp.int32, (rows, lanes), 1)
-    parts = [block_ref[s, start : start + rows, :] for s in range(4)]
+    notes = [block_ref[s, 3 * rows : 3 * rows + 8, :].astype(jnp.float32) for s in range(4)]
+    left = by_lane([note[matrix : matrix + 1, :] for note in notes], 0)
+    back = jnp.ones_like(left)
+    for b in STEPS:
+        holds = left >= b
+        back = jnp.where(holds, back * 2.0**-b, back)
+        left = jnp.where(holds, left - b, left)
+    back = back.astype(jnp.bfloat16)
+    parts = [block_ref[s, matrix * rows : (matrix + 1) * rows, :] for s in range(4)]
     for g in range(4):
-        merged = parts[(3 - g) % 4]
-        for p in (2, 1, 0):
-            merged = jnp.where(place < (p + 1) * width, parts[(p - g) % 4], merged)
+        merged = by_lane(parts, g)
         if g:
             merged = jnp.concatenate([merged[:, g * width :], merged[:, : g * width]], axis=1)
-        out_ref[g * rows : (g + 1) * rows, :] = merged
+        out_ref[g * rows : (g + 1) * rows, :] = merged * back
 
 
 def product_kernel(
-    both_ref,
-    third_ref,
+    blocks_ref,
     chosen_ref,
     gate_ref,
     up_ref,
+    down_ref,
     partial_ref,
-    down_ref,
     hidden_ref,
     gate_sum,
     up_sum,
+    turned_ref,
 ):
     i = pl.program_id(0)
-    steps = both_ref.shape[0] // 4
+    steps = blocks_ref.shape[0] // 4
     lanes = gate_ref.shape[1]
-    rows = gate_ref.shape[0] // 4
 
     @pl.when(i < steps)
     def _():
-        unpack(both_ref.at[pl.ds(4 * i, 4)], 0, gate_ref)
-        unpack(both_ref.at[pl.ds(4 * i, 4)], rows, up_ref)
+        unpack(blocks_ref.at[pl.ds(4 * i, 4)], 0, gate_ref)
+        unpack(blocks_ref.at[pl.ds(4 * i, 4)], 1, up_ref)
         chosen = chosen_ref[:, pl.ds(pl.multiple_of(i * lanes, 128), lanes)]
         gate = lax.dot_general(chosen, gate_ref[...], LAST, preferred_element_type=jnp.float32)
         up = lax.dot_general(chosen, up_ref[...], LAST, preferred_element_type=jnp.float32)
@@ -105,13 +118,19 @@
 
     @pl.when(i >= steps)
     def _():
-        unpack(third_ref.at[pl.ds(4 * (i - steps), 4)], 0, down_ref)
+        j = i - steps
+        unpack(blocks_ref.at[pl.ds(4 * j, 4)], 2, down_ref)
         product = jnp.dot(hidden_ref[...], down_ref[...], preferred_element_type=jnp.float32)
-        partial_ref[...] = product.T.astype(jnp.bfloat16)
-
-
-def output_kernel(third_ref, down_ref):
-    unpack(third_ref.at[pl.ds(4 * pl.program_id(0), 4)], 0, down_ref)
+        turned_ref[pl.ds(pl.multiple_of(j * lanes, 128), lanes), :] = product.T
+
+    @pl.when(i == 2 * steps - 1)
+    def _():
+        third = partial_ref.shape[1]
+        for d in range(partial_ref.shape[0]):
+            pieces = [
+                turned_ref[(3 * d + g) * third : (3 * d + g + 1) * third, :] for g in range(3)
+            ]
+            partial_ref[d] = jnp.concatenate(pieces, axis=1).astype(jnp.bfloat16)
 
 
 def combine_kernel(received_ref, routes_ref, weights_ref, mixed_ref):
@@ -120,13 +139,16 @@
     routes = routes_ref[...]
     rows = routes.shape[1]
     _, rank = ranks(routes, experts)
-    width = received_ref.shape[1]
+    width = 3 * received_ref.shape[1]
     slots = lax.broadcasted_iota(jnp.int32, (CAP, rows), 0).astype(jnp.float32)
     totals = [jnp.zeros((width, rows), jnp.float32) for _ in range(2)]
     for e in range(experts):
-        summed = received_ref[e * slices].astype(jnp.float32)
+        beside = received_ref[e * slices].astype(jnp.float32)
         for s in range(1, slices):
-            summed = summed + received_ref[e * slices + s].astype(jnp.float32)
+            beside = beside + received_ref[e * slices + s].astype(jnp.float32)
+        summed = jnp.concatenate(
+            [beside[:, g * CAP : (g + 1) * CAP] for g in range(3)], axis=0
+        )
         high = summed.astype(jnp.bfloat16)
         low = (summed - high.astype(jnp.float32)).astype(jnp.bfloat16)
         at = slots == rank[e : e + 1, :]
@@ -199,70 +221,39 @@
         factor = jnp.where(fits, factor * 2.0**b, factor)
         power = jnp.where(fits, power + b, power)
     sent = (wide * factor[:, None, None]).astype(jnp.float16).reshape(3 * quarter, lanes)
-    note = jnp.broadcast_to(power[:, None], (3, lanes // 3)).reshape(1, lanes)
-    note = jnp.broadcast_to(note, (8, lanes)).astype(jnp.float16)
+    note = jnp.concatenate([power, jnp.zeros((5,), jnp.float32)])
+    note = jnp.broadcast_to(note[:, None], (8, lanes)).astype(jnp.float16)
     gathered = lax.all_gather(jnp.concatenate([sent, note], axis=0), "fs", axis=0)
-    left = jnp.stack(
-        [gathered[:, 3 * quarter, m * (lanes // 3)] for m in range(3)], axis=1
-    ).astype(jnp.float32)
-    back = jnp.ones_like(left)
-    for b in STEPS:
-        holds = left >= b
-        back = jnp.where(holds, back * 2.0**-b, back)
-        left = jnp.where(holds, left - b, left)
-
-    def returned(start, stop):
-        part = gathered[:, start * quarter : stop * quarter].astype(jnp.float32)
-        part = part.reshape(fs_count, stop - start, quarter, lanes)
-        part = (part * back[:, start:stop, None, None]).astype(jnp.bfloat16)
-        return part.reshape(fs_count, (stop - start) * quarter, lanes)
-
-    both = returned(0, 2)
-    third = returned(2, 3)
+    blocks = gathered.astype(jnp.bfloat16)
     steps = fs_count // 4
     whole = pl.BlockSpec(memory_space=pltpu.VMEM)
     matrix = jax.ShapeDtypeStruct((block_rows, width), jnp.bfloat16)
-    held = pl.BlockSpec((block_rows, lanes), lambda i: (0, jnp.minimum(i, steps - 1)))
-    gate_new, up_new, partial = pl.pallas_call(
+    early = pl.BlockSpec((block_rows, lanes), lambda i: (0, jnp.minimum(i, steps - 1)))
+    late = pl.BlockSpec((block_rows, lanes), lambda i: (0, jnp.maximum(i - steps, 0)))
+    third = width // tp_count // 3
+    gate_new, up_new, down_new, partial = pl.pallas_call(
         product_kernel,
         grid=(2 * steps,),
-        out_shape=(matrix, matrix, jax.ShapeDtypeStruct((width, CAP), jnp.bfloat16)),
-        in_specs=[whole] * 3,
-        out_specs=(
-            held,
-            held,
-            pl.BlockSpec((lanes, CAP), lambda i: (jnp.maximum(i - steps, 0), 0)),
+        out_shape=(
+            matrix,
+            matrix,
+            matrix,
+            jax.ShapeDtypeStruct((tp_count, third, 3 * CAP), jnp.bfloat16),
         ),
+        in_specs=[whole] * 2,
+        out_specs=(early, early, late, whole),
         scratch_shapes=[
-            pltpu.VMEM((block_rows, lanes), jnp.bfloat16),
             pltpu.VMEM((CAP, block_rows), jnp.bfloat16),
             pltpu.VMEM((CAP, block_rows), jnp.float32),
             pltpu.VMEM((CAP, block_rows), jnp.float32),
+            pltpu.VMEM((width, CAP), jnp.float32),
         ],
         compiler_params=pltpu.CompilerParams(vmem_limit_bytes=24 * 2**20),
         cost_estimate=pl.CostEstimate(
             flops=3 * 2 * CAP * block_rows * width, bytes_accessed=2**23, transcendentals=0
         ),
-    )(both, third, chosen)
-    down_new = pl.pallas_call(
-        output_kernel,
-        grid=(steps,),
-        out_shape=matrix,
-        in_specs=[whole],
-        out_specs=pl.BlockSpec((block_rows, lanes), lambda i: (0, i)),
-        compiler_params=pltpu.CompilerParams(vmem_limit_bytes=24 * 2**20),
-        cost_estimate=pl.CostEstimate(
-            flops=5000000000, bytes_accessed=2**24, transcendentals=0
-        ),
-    )(third)
-
-    received = lax.all_to_all(
-        partial.reshape(tp_count, width // tp_count, CAP),
-        "tp",
-        split_axis=0,
-        concat_axis=0,
-        tiled=True,
-    )
+    )(blocks, chosen)
+    received = lax.all_to_all(partial, "tp", split_axis=0, concat_axis=0, tiled=True)
     mixed = pl.pallas_call(
         combine_kernel,
         out_shape=jax.ShapeDtypeStruct((width // tp_count, rows), jnp.bfloat16),

time: 140 us -> 128 us (0.914)
  blocking collectives: 70.3 us -> 87.3 us
  waiting for transfers between devices: 24.6 us -> 11.6 us
  other arithmetic: 10.7 us -> 5.9 us
  starting transfers between devices: 14.7 us -> 10.5 us
  local copies, waits for them, and re-layouts: 4.92 us -> 0.78 us
  Pallas kernels: 12.9 us -> 11.2 us
    all_to_all x0 -> x1, blocking collectives: none -> 18.4 us  [shards(): lax.all_to_all(partial, 'tp', split_axis=0, concat_axis=0, tiled=True)]
    all_to_all x1 -> x0, waiting for transfers between devices: 14.8 us -> none  [shards(): lax.all_to_all(partial.reshape(tp_count, width // tp_count, CAP), 'tp', s...]
    convert_element_type x3 -> x1, other arithmetic: 6.51 us -> 1.49 us  [shards(): blocks = gathered.astype(jnp.bfloat16)]
    all_to_all x1 -> x0, starting transfers between devices: 4.2 us -> none  [shards(): lax.all_to_all(partial.reshape(tp_count, width // tp_count, CAP), 'tp', s...]
    pallas_call x1 -> x0, Pallas kernels: 3.02 us -> none  [shards(): pl.pallas_call(output_kernel, grid=(steps,), out_shape=matrix, in_specs=[...]
    unnamed x10 -> x6, local copies, waits for them, and re-layouts: 2.67 us -> 0.01 us
    all_to_all x1, waiting for transfers between devices: 9.8 us -> 11.6 us  [shards(): lax.all_to_all(jnp.concatenate(pieces, axis=1), 'tp', split_axis=0, conca...]
  transfers between devices with their start and end apart: 2 -> 1, of which waited for: 2 -> 1; matrix products, arithmetic and copies ran while one was open for 0% -> 0% of each run, Pallas kernels for 3% -> 0%
where the time goes in v3:
time: 128 us
  blocking collectives  87.3 us (68%)
  waiting for transfers between devices  11.6 us (9%)
  Pallas kernels  11.2 us (9%)
  starting transfers between devices  10.5 us (8%)
  other arithmetic  5.9 us (5%)
    all_gather x1, blocking collectives, shards(): lax.all_gather(jnp.concatenate([sent, note], axis=0), 'fs', axis=0)  68.9 us
    all_to_all x1, blocking collectives, shards(): lax.all_to_all(partial, 'tp', split_axis=0, concat_axis=0, tiled=True)  18.4 us
    all_to_all x1, waiting for transfers between devices, shards(): lax.all_to_all(jnp.concatenate(pieces, axis=1), 'tp', split_axis=0, conca...  11.6 us
    all_to_all x1, starting transfers between devices, shards(): lax.all_to_all(jnp.concatenate(pieces, axis=1), 'tp', split_axis=0, conca...  10.5 us
    pallas_call x1, Pallas kernels, shards(): pl.pallas_call(product_kernel, grid=(2 * steps,), out_shape=(matrix, matr...  9.35 us
  transfers between devices with their start and end apart: 1, of which 1 were waited for; matrix products, arithmetic and copies ran while one was open for 0% of the time, Pallas kernels for 0%

profile of v3, /device:TPU:1, one launch (start us, length us, event | category | flops | bytes accessed | tf_op | source)
XLA Modules:
  0.0 128.0 jit_solution(3606451896783677374)
XLA Ops:
  0.6 0.0 copy-start
  0.6 0.0 copy-start.2
  0.7 1.1 convert_bitcast_fusion
  1.7 0.1 reshape.69
  1.8 1.1 fusion.5
  2.9 0.1 reshape.67
  3.0 0.1 reshape.68
  3.0 1.0 pad_maximum_fusion
  4.0 10.5 %all-to-all-start = ((bf16[32,54,96]{2,1,0:T(8,128)(2,1)}), bf16[32,54,96]{2,1,0:T(8,128)(2,1)S(1)}, u32[]{:S(2)}, u32[]{:S(2)}) async-start(bf16[32,54,96]{2,1,0:T(8,128)(2,1)} %pad_maximum_fusion), calls=%async_computation | async-start | bytes 917504 | tf_op jit(solution)/shard_map/all_to_all | solution.py:180
  14.5 0.0 copy-done
  14.5 0.0 copy-done.2
  14.5 0.5 shard_map.102.chosen_ref
  15.1 11.6 %all-to-all-done = bf16[32,54,96]{2,1,0:T(8,128)(2,1)S(1)} async-done(((bf16[32,54,96]{2,1,0:T(8,128)(2,1)}), bf16[32,54,96]{2,1,0:T(8,128)(2,1)S(1)}, u32[]{:S(2)}, u32[]{:S(2)}) %all-to-all-start) | async-done | bytes 331808 | tf_op jit(solution)/shard_map/all_to_all | solution.py:180
  26.7 0.1 fusion.9
  26.9 0.1 stack_reshape.11
  26.9 0.1 stack_reshape.10
  27.0 0.1 stack_reshape.9
  27.1 0.4 fusion.2
  27.5 0.1 slice_bitcast_fusion.3
  27.6 0.3 abs_reduce_fusion
  27.9 0.1 fusion.7
  28.0 0.1 mul.182
  28.1 0.1 mul.183
  28.2 0.3 multiply_convert_fusion
  28.5 0.1 pad_maximum_fusion.1
  28.6 68.9 %all-gather.2 = f16[10560,384]{1,0:T(8,128)(2,1)S(1)} all-gather(f16[440,384]{1,0:T(8,128)(2,1)S(1)} %pad_maximum_fusion.1), channel_id=2, replica_groups=mesh['fs'=24,'tp'=32] {'fs'}, dimensions={0}, use_global_device_ids=true | all-gather | bytes 8448000 | tf_op jit(solution)/shard_map/all_gather | solution.py:226
  97.5 1.5 %convert_element_type.31 = bf16[10560,384]{1,0:T(8,128)(2,1)S(1)} convert(f16[10560,384]{1,0:T(8,128)(2,1)S(1)} %all-gather.2) | non-fusion elementwise | flops 4055040 | bytes 16220160 | tf_op jit(solution)/shard_map/convert_element_type | solution.py:227
  99.0 0.0 copy-start.1
  99.0 9.4 %shard_map.103 = (bf16[576,2304]{1,0:T(8,128)(2,1)}, bf16[576,2304]{1,0:T(8,128)(2,1)}, bf16[576,2304]{1,0:T(8,128)(2,1)}, bf16[32,24,216]{2,1,0:T(8,128)(2,1)S(1)}) custom-call(bf16[24,440,384]{2,1,0:T(8,128)(2,1)S(1)} %bitcast.35, bf16[72,2304]{1,0:T(8,128)(2,1)S(1)} %shard_map.102.chosen_ref), custom_call_target="tpu_custom_call" | custom-call | flops 573308928 | bytes 8388608 | tf_op jit(solution)/shard_map/pallas_call | solution.py:234
  108.4 18.4 %all_to_all.10.received_ref = bf16[32,24,216]{2,1,0:T(8,128)(2,1)S(1)} all-to-all(bf16[32,24,216]{2,1,0:T(8,128)(2,1)S(1)} %get-tuple-element.11), channel_id=1, replica_groups=mesh['fs'=24,'tp'=32] {'tp'}, dimensions={0} | all-to-all | bytes 663552 | tf_op jit(solution)/shard_map/all_to_all | solution.py:256
  126.8 0.0 copy-done.1
  126.8 1.3 shard_map.104
  (2 shorter events, 0.0 us)
Async XLA Ops:
  0.6 13.9 %copy-start = (s32[192,2]{0,1:T(2,128)S(1)}, s32[192,2]{0,1:T(2,128)}, u32[]{:S(2)}) copy-start(s32[192,2]{0,1:T(2,128)} %param.12) | copy-start | bytes 4612
  0.6 13.9 %copy-start.2 = (bf16[192,2304]{1,0:T(8,128)(2,1)S(1)}, bf16[192,2304]{1,0:T(8,128)(2,1)}, u32[]{:S(2)}) copy-start(bf16[192,2304]{1,0:T(8,128)(2,1)} %tokens_ref.1) | copy-start | bytes 2654212
  4.0 22.7 %all-to-all-start = ((bf16[32,54,96]{2,1,0:T(8,128)(2,1)}), bf16[32,54,96]{2,1,0:T(8,128)(2,1)S(1)}, u32[]{:S(2)}, u32[]{:S(2)}) async-start(bf16[32,54,96]{2,1,0:T(8,128)(2,1)} %pad_maximum_fusion), calls=%async_computation | async-start | bytes 917504 | tf_op jit(solution)/shard_map/all_to_all | solution.py:180
  99.0 27.7 %copy-start.1 = (f32[192,2]{0,1:T(2,128)S(1)}, f32[192,2]{0,1:T(2,128)}, u32[]{:S(2)}) copy-start(f32[192,2]{0,1:T(2,128)} %param.13) | copy-start | bytes 4612

commit v4 on v3

--- a/solution.py
+++ b/solution.py
@@ -11,11 +11,29 @@
 LAST = (((1,), (1,)), ((), ()))
 
 
-def arrange(matrix, tp_count):
-    experts, rows, cols = matrix.shape
-    slices = tp_count // experts
-    turned = matrix.transpose(0, 2, 1)
-    return turned.reshape(tp_count, cols // slices, rows)
+def arrange_kernel(gate_hbm, up_hbm, down_hbm, gain_ref, out_ref, held, arrived):
+    _, experts, units, _ = held.shape
+    slices = out_ref.shape[0] // experts
+    part = units // slices
+    half = experts // 2
+    copies = []
+    for h in range(2):
+        for m, source in enumerate((gate_hbm, up_hbm, down_hbm)):
+            chosen = pl.ds(h * half, half)
+            copy = pltpu.make_async_copy(
+                source.at[chosen], held.at[m, chosen], arrived.at[h, m]
+            )
+            copy.start()
+            copies.append(copy)
+    gain = gain_ref[...]
+    for e in range(experts):
+        if e % half == 0:
+            for copy in copies[3 * (e // half) : 3 * (e // half) + 3]:
+                copy.wait()
+        for s in range(slices):
+            rows = slice(s * part, (s + 1) * part)
+            pieces = [held[0, e, rows, :] * gain, held[1, e, rows, :] * gain, held[2, e, rows, :]]
+            out_ref[e * slices + s] = jnp.concatenate(pieces, axis=0).astype(jnp.bfloat16)
 
 
 def ranks(routes_t, experts):
@@ -48,33 +66,87 @@
     )
 
 
-def by_lane(parts, shift):
-    lanes = parts[0].shape[1]
-    place = lax.broadcasted_iota(jnp.int32, parts[0].shape, 1)
-    merged = parts[(3 - shift) % 4]
-    for p in (2, 1, 0):
-        merged = jnp.where(place < (p + 1) * (lanes // 4), parts[(p - shift) % 4], merged)
-    return merged
-
-
-def unpack(block_ref, matrix, out_ref):
+def pack_kernel(place_ref, moved_ref, out_ref, held):
+    sources, units, _ = moved_ref.shape
+    part = units // 3
+    rows = held.shape[2]
+    each = sources // 4
+    largest = [None] * 3
+    for g in range(4):
+        wide = [moved_ref[g * each + c].astype(jnp.float32) for c in range(each)]
+        for m in range(3):
+            group = jnp.concatenate([w[m * part : (m + 1) * part, :] for w in wide], axis=0)
+            held[m, g] = group
+            top = jnp.max(jnp.max(jnp.abs(group), axis=0, keepdims=True), axis=1, keepdims=True)
+            largest[m] = top if g == 0 else jnp.maximum(largest[m], top)
+    factors = []
+    note = jnp.zeros((8, out_ref.shape[1]), jnp.float32)
+    line = lax.broadcasted_iota(jnp.int32, note.shape, 0)
+    for m in range(3):
+        factor = jnp.ones((1, 1), jnp.float32)
+        power = jnp.zeros((1, 1), jnp.float32)
+        for b in STEPS:
+            fits = largest[m] * factor * 2.0**b <= 32768.0
+            factor = jnp.where(fits, factor * 2.0**b, factor)
+            power = jnp.where(fits, power + b, power)
+        factors.append(factor)
+        note = jnp.where(line == m, power, note)
+    out_ref[3 * rows : 3 * rows + 8, :] = note.astype(jnp.bfloat16)
+    for v in range(4):
+
+        @pl.when(place_ref[0] == v)
+        def _():
+            for m in range(3):
+                beside = jnp.concatenate([held[m, (p - v) % 4] for p in range(4)], axis=1)
+                out_ref[m * rows : (m + 1) * rows, :] = (beside * factors[m]).astype(jnp.bfloat16)
+
+
+def scales(blocks_ref, back_ref):
+    lanes = blocks_ref.shape[2]
+    width = lanes // 4
+    first = blocks_ref.shape[1] - 8
+    place = lax.broadcasted_iota(jnp.int32, (8, lanes), 1)
+    for i in range(blocks_ref.shape[0] // 4):
+        notes = [blocks_ref[4 * i + s, first:, :].astype(jnp.float32) for s in range(4)]
+        left = notes[3]
+        for s in (2, 1, 0):
+            left = jnp.where(place < (s + 1) * width, notes[s], left)
+        back = jnp.ones_like(left)
+        for b in STEPS:
+            holds = left >= b
+            back = jnp.where(holds, back * 2.0**-b, back)
+            left = jnp.where(holds, left - b, left)
+        back_ref[:, i * lanes : (i + 1) * lanes] = back
+
+
+def unpack(block_ref, matrix, back, out_ref, start):
     rows = out_ref.shape[0] // 4
-    lanes = out_ref.shape[1]
-    width = lanes // 4
-    notes = [block_ref[s, 3 * rows : 3 * rows + 8, :].astype(jnp.float32) for s in range(4)]
-    left = by_lane([note[matrix : matrix + 1, :] for note in notes], 0)
-    back = jnp.ones_like(left)
-    for b in STEPS:
-        holds = left >= b
-        back = jnp.where(holds, back * 2.0**-b, back)
-        left = jnp.where(holds, left - b, left)
+    lane = lax.broadcasted_iota(jnp.int32, (rows, 128), 1)
+    below = {n: lane < n for n in (32, 64, 96)}
     back = back.astype(jnp.bfloat16)
-    parts = [block_ref[s, matrix * rows : (matrix + 1) * rows, :] for s in range(4)]
+    tiles = [
+        [
+            block_ref[s, matrix * rows : (matrix + 1) * rows, 128 * t : 128 * (t + 1)]
+            for t in range(3)
+        ]
+        for s in range(4)
+    ]
     for g in range(4):
-        merged = by_lane(parts, g)
+        merged = [
+            jnp.where(below[96 - 32 * t], tiles[(t - g) % 4][t], tiles[(t + 1 - g) % 4][t])
+            for t in range(3)
+        ]
         if g:
-            merged = jnp.concatenate([merged[:, g * width :], merged[:, : g * width]], axis=1)
-        out_ref[g * rows : (g + 1) * rows, :] = merged * back
+            skip, by = divmod(96 * g, 128)
+            turned = [jnp.concatenate([m[:, by:], m[:, :by]], axis=1) for m in merged]
+            merged = [
+                jnp.where(below[128 - by], turned[(t + skip) % 3], turned[(t + skip + 1) % 3])
+                for t in range(3)
+            ]
+        for t in range(3):
+            out_ref[
+                g * rows : (g + 1) * rows, start + 128 * t : start + 128 * (t + 1)
+            ] = merged[t] * back[:, 128 * t : 128 * (t + 1)]
 
 
 def product_kernel(
@@ -88,16 +160,35 @@
     gate_sum,
     up_sum,
     turned_ref,
+    back_ref,
 ):
     i = pl.program_id(0)
-    steps = blocks_ref.shape[0] // 4
-    lanes = gate_ref.shape[1]
+    steps = pl.num_programs(0) // 2
+    lanes = blocks_ref.shape[2]
+    wide = gate_ref.shape[1]
+    inner = wide // lanes
+
+    @pl.when(i == 0)
+    def _():
+        scales(blocks_ref, back_ref)
+
+    def place(step, matrix, out_ref):
+        columns = pl.ds(pl.multiple_of(step * wide, 128), wide)
+        back = back_ref[:, columns]
+        for n in range(inner):
+            unpack(
+                blocks_ref.at[pl.ds(4 * (step * inner + n), 4)],
+                matrix,
+                back[matrix : matrix + 1, n * lanes : (n + 1) * lanes],
+                out_ref,
+                n * lanes,
+            )
 
     @pl.when(i < steps)
     def _():
-        unpack(blocks_ref.at[pl.ds(4 * i, 4)], 0, gate_ref)
-        unpack(blocks_ref.at[pl.ds(4 * i, 4)], 1, up_ref)
-        chosen = chosen_ref[:, pl.ds(pl.multiple_of(i * lanes, 128), lanes)]
+        place(i, 0, gate_ref)
+        place(i, 1, up_ref)
+        chosen = chosen_ref[:, pl.ds(pl.multiple_of(i * wide, 128), wide)]
         gate = lax.dot_general(chosen, gate_ref[...], LAST, preferred_element_type=jnp.float32)
         up = lax.dot_general(chosen, up_ref[...], LAST, preferred_element_type=jnp.float32)
 
@@ -119,9 +210,9 @@
     @pl.when(i >= steps)
     def _():
         j = i - steps
-        unpack(blocks_ref.at[pl.ds(4 * j, 4)], 2, down_ref)
+        place(j, 2, down_ref)
         product = jnp.dot(hidden_ref[...], down_ref[...], preferred_element_type=jnp.float32)
-        turned_ref[pl.ds(pl.multiple_of(j * lanes, 128), lanes), :] = product.T
+        turned_ref[pl.ds(pl.multiple_of(j * wide, 128), wide), :] = product.T
 
     @pl.when(i == 2 * steps - 1)
     def _():
@@ -171,14 +262,28 @@
     fs_count = lax.axis_size("fs")
     experts, features, _ = gate_train.shape
     slices = tp_count // experts
-    gain_column = gain[None, :, None]
-    gate_round = (gate_train * gain_column).astype(jnp.bfloat16)
-    up_round = (up_train * gain_column).astype(jnp.bfloat16)
-    down_round = down_train.astype(jnp.bfloat16)
-    pieces = [arrange(a, tp_count) for a in (gate_round, up_round, down_round)]
-    units = pieces[0].shape[1]
+    units = gate_train.shape[2] // slices
     moved = lax.all_to_all(
-        jnp.concatenate(pieces, axis=1), "tp", split_axis=0, concat_axis=0, tiled=True
+        pl.pallas_call(
+            arrange_kernel,
+            out_shape=jax.ShapeDtypeStruct((tp_count, 3 * units, features), jnp.bfloat16),
+            in_specs=[pl.BlockSpec(memory_space=pltpu.MemorySpace.HBM)] * 3
+            + [pl.BlockSpec(memory_space=pltpu.VMEM)],
+            scratch_shapes=[
+                pltpu.VMEM((3, experts, slices * units, features), jnp.float32),
+                pltpu.SemaphoreType.DMA((2, 3)),
+            ],
+            compiler_params=pltpu.CompilerParams(vmem_limit_bytes=60 * 1024 * 2**10),
+        )(
+            gate_train.transpose(0, 2, 1),
+            up_train.transpose(0, 2, 1),
+            down_train.transpose(0, 2, 1),
+            gain[None, :],
+        ),
+        "tp",
+        split_axis=0,
+        concat_axis=0,
+        tiled=True,
     )
 
     expert = (lax.axis_index("tp") // slices).astype(jnp.int32).reshape(1)
@@ -200,36 +305,26 @@
 
     block_rows = tp_count * units
     quarter = block_rows // 4
-    grouped = jnp.stack(
-        [
-            moved[:, m * units : (m + 1) * units].reshape(4, quarter, features)
-            for m in range(3)
+    lanes = 4 * features
+    packed = pl.pallas_call(
+        pack_kernel,
+        out_shape=jax.ShapeDtypeStruct((3 * quarter + 8, lanes), jnp.bfloat16),
+        in_specs=[
+            pl.BlockSpec(memory_space=pltpu.SMEM),
+            pl.BlockSpec(memory_space=pltpu.VMEM),
         ],
-        axis=1,
-    )
-    shift = (4 - lax.axis_index("fs") % 4) % 4
-    turned = lax.dynamic_slice_in_dim(jnp.concatenate([grouped, grouped], axis=0), shift, 4, 0)
-    packed = jnp.concatenate([turned[p] for p in range(4)], axis=-1)
-    lanes = 4 * features
-
-    wide = packed.astype(jnp.float32)
-    largest = jnp.max(jnp.abs(wide), axis=(1, 2))
-    factor = jnp.ones_like(largest)
-    power = jnp.zeros_like(largest)
-    for b in STEPS:
-        fits = largest * factor * 2.0**b <= 32768.0
-        factor = jnp.where(fits, factor * 2.0**b, factor)
-        power = jnp.where(fits, power + b, power)
-    sent = (wide * factor[:, None, None]).astype(jnp.float16).reshape(3 * quarter, lanes)
-    note = jnp.concatenate([power, jnp.zeros((5,), jnp.float32)])
-    note = jnp.broadcast_to(note[:, None], (8, lanes)).astype(jnp.float16)
-    gathered = lax.all_gather(jnp.concatenate([sent, note], axis=0), "fs", axis=0)
+        out_specs=pl.BlockSpec(memory_space=pltpu.VMEM),
+        scratch_shapes=[pltpu.VMEM((3, 4, quarter, features), jnp.float32)],
+        compiler_params=pltpu.CompilerParams(vmem_limit_bytes=24 * 2**20),
+    )((lax.axis_index("fs") % 4).astype(jnp.int32).reshape(1), moved)
+    gathered = lax.all_gather(packed.astype(jnp.float16), "fs", axis=0)
     blocks = gathered.astype(jnp.bfloat16)
-    steps = fs_count // 4
+    steps = fs_count // 8
+    wide = width // steps
     whole = pl.BlockSpec(memory_space=pltpu.VMEM)
     matrix = jax.ShapeDtypeStruct((block_rows, width), jnp.bfloat16)
-    early = pl.BlockSpec((block_rows, lanes), lambda i: (0, jnp.minimum(i, steps - 1)))
-    late = pl.BlockSpec((block_rows, lanes), lambda i: (0, jnp.maximum(i - steps, 0)))
+    early = pl.BlockSpec((block_rows, wide), lambda i: (0, jnp.minimum(i, steps - 1)))
+    late = pl.BlockSpec((block_rows, wide), lambda i: (0, jnp.maximum(i - steps, 0)))
     third = width // tp_count // 3
     gate_new, up_new, down_new, partial = pl.pallas_call(
         product_kernel,
@@ -247,6 +342,7 @@
             pltpu.VMEM((CAP, block_rows), jnp.float32),
             pltpu.VMEM((CAP, block_rows), jnp.float32),
             pltpu.VMEM((width, CAP), jnp.float32),
+            pltpu.VMEM((8, width), jnp.float32),
         ],
         compiler_params=pltpu.CompilerParams(vmem_limit_bytes=24 * 2**20),
         cost_estimate=pl.CostEstimate(

time: 128 us -> 124 us (0.969)
  other arithmetic: 5.9 us -> 1.55 us
  waiting for transfers between devices: 11.6 us -> 9.82 us
    pallas_call x0 -> x2, Pallas kernels: none -> 3.32 us  [the longest x1 2.77 us: shards(): pl.pallas_call(arrange_kernel, out_shape=jax.ShapeDtypeStruct((tp_count,...]
    pallas_call x1, Pallas kernels: 9.35 us -> 7.01 us  [shards(): pl.pallas_call(product_kernel, grid=(2 * steps,), out_shape=(matrix, matr...]
    transpose x2 -> x0, other arithmetic: 2.18 us -> none  [arrange(): turned = matrix.transpose(0, 2, 1)]
    unnamed x6 -> x8, local copies, waits for them, and re-layouts: 0.01 us -> 1.86 us
    all_to_all x1, waiting for transfers between devices: 11.6 us -> 9.82 us  [shards(): lax.all_to_all(pl.pallas_call(arrange_kernel, out_shape=jax.ShapeDtypeStr...]
    concatenate x4 -> x0, other arithmetic: 1.56 us -> none  [the longest x1 0.96 us: shards(): jnp.concatenate(pieces, axis=1)]
where the time goes in v4:
time: 124 us
  blocking collectives  87.3 us (70%)
  Pallas kernels  12.1 us (10%)
  starting transfers between devices  10.5 us (8%)
  waiting for transfers between devices  9.82 us (8%)
  local copies, waits for them, and re-layouts  1.86 us (2%)
  other arithmetic  1.55 us (1%)
    all_gather x1, blocking collectives, shards(): gathered = lax.all_gather(packed.astype(jnp.float16), 'fs', axis=0)  68.9 us
    all_to_all x1, blocking collectives, shards(): lax.all_to_all(partial, 'tp', split_axis=0, concat_axis=0, tiled=True)  18.4 us
    all_to_all x1, starting transfers between devices, shards(): lax.all_to_all(pl.pallas_call(arrange_kernel, out_shape=jax.ShapeDtypeStr...  10.5 us
    all_to_all x1, waiting for transfers between devices, shards(): lax.all_to_all(pl.pallas_call(arrange_kernel, out_shape=jax.ShapeDtypeStr...  9.82 us
    pallas_call x1, Pallas kernels, shards(): pl.pallas_call(product_kernel, grid=(2 * steps,), out_shape=(matrix, matr...  7.01 us
    pallas_call x1, Pallas kernels, shards(): pl.pallas_call(arrange_kernel, out_shape=jax.ShapeDtypeStruct((tp_count,...  2.77 us
  transfers between devices with their start and end apart: 1, of which 1 were waited for; matrix products, arithmetic and copies ran while one was open for 0% of the time, Pallas kernels for 0%

profile of v4, /device:TPU:1, one launch (start us, length us, event | category | flops | bytes accessed | tf_op | source)
XLA Modules:
  0.0 123.9 jit_solution(16468084782180400440)
XLA Ops:
  0.6 2.8 %shard_map.102 = bf16[32,54,96]{2,1,0:T(8,128)(2,1)} custom-call(f32[8,72,96]{2,1,0:T(8,128)} %bitcast.17, f32[8,72,96]{2,1,0:T(8,128)} %bitcast.18, f32[8,72,96]{2,1,0:T(8,128)} %bitcast.19, f32[1,96]{1,0:T(1,128)} %bitcast.21), custom_call_target="tpu_custom_call" | custom-call | tf_op jit(solution)/shard_map/pallas_call | solution.py:267
  3.4 10.5 %all-to-all-start = ((bf16[32,54,96]{2,1,0:T(8,128)(2,1)}), bf16[32,54,96]{2,1,0:T(8,128)(2,1)S(1)}, u32[]{:S(2)}, u32[]{:S(2)}) async-start(bf16[32,54,96]{2,1,0:T(8,128)(2,1)} %shard_map.102), calls=%async_computation | async-start | bytes 917504 | tf_op jit(solution)/shard_map/all_to_all | solution.py:266
  13.9 0.0 copy-start
  14.0 0.7 copy-done
  14.6 0.0 copy-start.3
  14.6 1.2 copy-done.3
  15.8 0.5 shard_map.104.chosen_ref
  16.3 9.8 %all-to-all-done.moved_ref = bf16[32,54,96]{2,1,0:T(8,128)(2,1)S(1)} async-done(((bf16[32,54,96]{2,1,0:T(8,128)(2,1)}), bf16[32,54,96]{2,1,0:T(8,128)(2,1)S(1)}, u32[]{:S(2)}, u32[]{:S(2)}) %all-to-all-start) | async-done | bytes 331808 | tf_op jit(solution)/shard_map/all_to_all | solution.py:266
  26.2 0.6 shard_map.103
  26.7 0.1 convert_element_type.6
  26.8 68.9 %all-gather.2 = f16[10560,384]{1,0:T(8,128)(2,1)S(1)} all-gather(f16[440,384]{1,0:T(8,128)(2,1)S(1)} %convert_element_type.6), channel_id=2, replica_groups=mesh['fs'=24,'tp'=32] {'fs'}, dimensions={0}, use_global_device_ids=true | all-gather | bytes 8448000 | tf_op jit(solution)/shard_map/all_gather | solution.py:320
  95.7 1.5 %convert_element_type.8 = bf16[10560,384]{1,0:T(8,128)(2,1)S(1)} convert(f16[10560,384]{1,0:T(8,128)(2,1)S(1)} %all-gather.2) | non-fusion elementwise | flops 4055040 | bytes 16220160 | tf_op jit(solution)/shard_map/convert_element_type | solution.py:321
  97.2 0.0 copy-start.1
  97.2 0.0 copy-start.2
  97.2 7.0 %shard_map.105 = (bf16[576,2304]{1,0:T(8,128)(2,1)}, bf16[576,2304]{1,0:T(8,128)(2,1)}, bf16[576,2304]{1,0:T(8,128)(2,1)}, bf16[32,24,216]{2,1,0:T(8,128)(2,1)S(1)}) custom-call(bf16[24,440,384]{2,1,0:T(8,128)(2,1)S(1)} %bitcast.13, bf16[72,2304]{1,0:T(8,128)(2,1)S(1)} %shard_map.104.chosen_ref), custom_call_target="tpu_custom_call" | custom-call | flops 573308928 | bytes 8388608 | tf_op jit(solution)/shard_map/pallas_call | solution.py:329
  104.2 18.4 %all_to_all.10.received_ref = bf16[32,24,216]{2,1,0:T(8,128)(2,1)S(1)} all-to-all(bf16[32,24,216]{2,1,0:T(8,128)(2,1)S(1)} %get-tuple-element.11), channel_id=1, replica_groups=mesh['fs'=24,'tp'=32] {'tp'}, dimensions={0} | all-to-all | bytes 663552 | tf_op jit(solution)/shard_map/all_to_all | solution.py:352
  122.6 0.0 copy-done.1
  122.6 0.0 copy-done.2
  122.6 1.3 %shard_map.106 = bf16[72,192]{1,0:T(8,128)(2,1)} custom-call(bf16[32,24,216]{2,1,0:T(8,128)(2,1)S(1)} %all_to_all.10.received_ref, s32[2,192]{1,0:T(2,128)S(1)} %bitcast.15, f32[2,192]{1,0:T(2,128)S(1)} %bitcast.16), custom_call_target="tpu_custom_call" | custom-call | tf_op jit(solution)/shard_map/pallas_call | solution.py:353
Async XLA Ops:
  3.4 22.8 %all-to-all-start = ((bf16[32,54,96]{2,1,0:T(8,128)(2,1)}), bf16[32,54,96]{2,1,0:T(8,128)(2,1)S(1)}, u32[]{:S(2)}, u32[]{:S(2)}) async-start(bf16[32,54,96]{2,1,0:T(8,128)(2,1)} %shard_map.102), calls=%async_computation | async-start | bytes 917504 | tf_op jit(solution)/shard_map/all_to_all | solution.py:266
  13.9 0.7 copy-start
  14.6 1.2 copy-start.3
  97.2 25.4 %copy-start.1 = (s32[192,2]{0,1:T(2,128)S(1)}, s32[192,2]{0,1:T(2,128)}, u32[]{:S(2)}) copy-start(s32[192,2]{0,1:T(2,128)} %param.12) | copy-start | bytes 4612
  97.2 25.4 %copy-start.2 = (f32[192,2]{0,1:T(2,128)S(1)}, f32[192,2]{0,1:T(2,128)}, u32[]{:S(2)}) copy-start(f32[192,2]{0,1:T(2,128)} %param.13) | copy-start | bytes 4612

commit v5 on v4

--- a/solution.py
+++ b/solution.py
@@ -26,6 +26,9 @@
             copy.start()
             copies.append(copy)
     gain = gain_ref[...]
+    features = gain.shape[1]
+    rest = 128 - features
+    gap = jnp.zeros((2, rest), jnp.float32)
     for e in range(experts):
         if e % half == 0:
             for copy in copies[3 * (e // half) : 3 * (e // half) + 3]:
@@ -33,7 +36,13 @@
         for s in range(slices):
             rows = slice(s * part, (s + 1) * part)
             pieces = [held[0, e, rows, :] * gain, held[1, e, rows, :] * gain, held[2, e, rows, :]]
-            out_ref[e * slices + s] = jnp.concatenate(pieces, axis=0).astype(jnp.bfloat16)
+            lines = jnp.concatenate(pieces, axis=0)
+            beside = []
+            for q in range(3):
+                beside += [lines[48:54, q * rest : (q + 1) * rest], gap]
+            upper = jnp.concatenate([lines[0:24], jnp.concatenate(beside, axis=0)], axis=1)
+            lower = jnp.concatenate([lines[24:48], jnp.zeros((24, rest), jnp.float32)], axis=1)
+            out_ref[e * slices + s] = jnp.concatenate([upper, lower], axis=0).astype(jnp.bfloat16)
 
 
 def ranks(routes_t, experts):
@@ -67,15 +76,21 @@
 
 
 def pack_kernel(place_ref, moved_ref, out_ref, held):
-    sources, units, _ = moved_ref.shape
-    part = units // 3
-    rows = held.shape[2]
+    sources = moved_ref.shape[0]
+    rows, features = held.shape[2:]
+    part = 4 * rows // sources
     each = sources // 4
     largest = [None] * 3
     for g in range(4):
         wide = [moved_ref[g * each + c].astype(jnp.float32) for c in range(each)]
         for m in range(3):
-            group = jnp.concatenate([w[m * part : (m + 1) * part, :] for w in wide], axis=0)
+            pieces = []
+            for w in wide:
+                pieces.append(w[m * part : min((m + 1) * part, 48), 0:features])
+                if m == 2:
+                    tail = [w[8 * q : 8 * q + 6, features:] for q in range(3)]
+                    pieces.append(jnp.concatenate(tail, axis=1))
+            group = jnp.concatenate(pieces, axis=0)
             held[m, g] = group
             top = jnp.max(jnp.max(jnp.abs(group), axis=0, keepdims=True), axis=1, keepdims=True)
             largest[m] = top if g == 0 else jnp.maximum(largest[m], top)
@@ -152,76 +167,78 @@
 def product_kernel(
     blocks_ref,
     chosen_ref,
-    gate_ref,
-    up_ref,
-    down_ref,
+    gate_hbm,
+    up_hbm,
+    down_hbm,
     partial_ref,
-    hidden_ref,
+    held,
     gate_sum,
     up_sum,
-    turned_ref,
+    result_ref,
     back_ref,
+    written,
 ):
-    i = pl.program_id(0)
-    steps = pl.num_programs(0) // 2
+    steps = written.shape[1]
     lanes = blocks_ref.shape[2]
-    wide = gate_ref.shape[1]
+    wide = held.shape[2] // steps
     inner = wide // lanes
-
-    @pl.when(i == 0)
-    def _():
-        scales(blocks_ref, back_ref)
-
-    def place(step, matrix, out_ref):
-        columns = pl.ds(pl.multiple_of(step * wide, 128), wide)
-        back = back_ref[:, columns]
+    outputs = (gate_hbm, up_hbm, down_hbm)
+    copies = []
+    scales(blocks_ref, back_ref)
+
+    def place(step, matrix):
         for n in range(inner):
+            at = step * wide + n * lanes
             unpack(
                 blocks_ref.at[pl.ds(4 * (step * inner + n), 4)],
                 matrix,
-                back[matrix : matrix + 1, n * lanes : (n + 1) * lanes],
-                out_ref,
-                n * lanes,
+                back_ref[matrix : matrix + 1, at : at + lanes],
+                held.at[matrix],
+                at,
             )
 
-    @pl.when(i < steps)
-    def _():
-        place(i, 0, gate_ref)
-        place(i, 1, up_ref)
-        chosen = chosen_ref[:, pl.ds(pl.multiple_of(i * wide, 128), wide)]
-        gate = lax.dot_general(chosen, gate_ref[...], LAST, preferred_element_type=jnp.float32)
-        up = lax.dot_general(chosen, up_ref[...], LAST, preferred_element_type=jnp.float32)
-
-        @pl.when(i == 0)
-        def _():
-            gate_sum[...] = gate
-            up_sum[...] = up
-
-        @pl.when(i > 0)
-        def _():
-            gate_sum[...] += gate
-            up_sum[...] += up
-
-    @pl.when(i == steps - 1)
-    def _():
-        total = gate_sum[...]
-        hidden_ref[...] = (total / (1.0 + jnp.exp(-total)) * up_sum[...]).astype(jnp.bfloat16)
-
-    @pl.when(i >= steps)
-    def _():
-        j = i - steps
-        place(j, 2, down_ref)
-        product = jnp.dot(hidden_ref[...], down_ref[...], preferred_element_type=jnp.float32)
-        turned_ref[pl.ds(pl.multiple_of(j * wide, 128), wide), :] = product.T
-
-    @pl.when(i == 2 * steps - 1)
-    def _():
-        third = partial_ref.shape[1]
-        for d in range(partial_ref.shape[0]):
-            pieces = [
-                turned_ref[(3 * d + g) * third : (3 * d + g + 1) * third, :] for g in range(3)
-            ]
-            partial_ref[d] = jnp.concatenate(pieces, axis=1).astype(jnp.bfloat16)
+    def write(step, matrix):
+        columns = pl.ds(step * wide, wide)
+        copy = pltpu.make_async_copy(
+            held.at[matrix, :, columns], outputs[matrix].at[:, columns], written.at[matrix, step]
+        )
+        copy.start()
+        copies.append(copy)
+
+    for i in range(steps):
+        columns = slice(i * wide, (i + 1) * wide)
+        place(i, 0)
+        place(i, 1)
+        chosen = chosen_ref[:, columns]
+        for matrix, total in ((0, gate_sum), (1, up_sum)):
+            part = lax.dot_general(
+                chosen, held[matrix, :, columns], LAST, preferred_element_type=jnp.float32
+            )
+            if i:
+                total[...] += part
+            else:
+                total[...] = part
+        write(i, 0)
+        write(i, 1)
+    gate = gate_sum[...]
+    hidden = (gate / (1.0 + jnp.exp(-gate)) * up_sum[...]).astype(jnp.bfloat16)
+    for i in range(steps):
+        columns = slice(i * wide, (i + 1) * wide)
+        place(i, 2)
+        result_ref[:, columns] = jnp.dot(
+            hidden, held[2, :, columns], preferred_element_type=jnp.float32
+        )
+        write(i, 2)
+
+    third = partial_ref.shape[1]
+    own = partial_ref.shape[2] // 3
+    for d in range(partial_ref.shape[0]):
+        pieces = [
+            result_ref[g * third : (g + 1) * third, d * own : (d + 1) * own] for g in range(3)
+        ]
+        partial_ref[d] = jnp.concatenate(pieces, axis=1).astype(jnp.bfloat16)
+    for copy in copies:
+        copy.wait()
 
 
 def combine_kernel(received_ref, routes_ref, weights_ref, mixed_ref):
@@ -230,7 +247,7 @@
     routes = routes_ref[...]
     rows = routes.shape[1]
     _, rank = ranks(routes, experts)
-    width = 3 * received_ref.shape[1]
+    width = received_ref.shape[2] // 3
     slots = lax.broadcasted_iota(jnp.int32, (CAP, rows), 0).astype(jnp.float32)
     totals = [jnp.zeros((width, rows), jnp.float32) for _ in range(2)]
     for e in range(experts):
@@ -238,8 +255,8 @@
         for s in range(1, slices):
             beside = beside + received_ref[e * slices + s].astype(jnp.float32)
         summed = jnp.concatenate(
-            [beside[:, g * CAP : (g + 1) * CAP] for g in range(3)], axis=0
-        )
+            [beside[:, g * width : (g + 1) * width] for g in range(3)], axis=0
+        ).T
         high = summed.astype(jnp.bfloat16)
         low = (summed - high.astype(jnp.float32)).astype(jnp.bfloat16)
         at = slots == rank[e : e + 1, :]
@@ -266,7 +283,7 @@
     moved = lax.all_to_all(
         pl.pallas_call(
             arrange_kernel,
-            out_shape=jax.ShapeDtypeStruct((tp_count, 3 * units, features), jnp.bfloat16),
+            out_shape=jax.ShapeDtypeStruct((tp_count, 48, 128), jnp.bfloat16),
             in_specs=[pl.BlockSpec(memory_space=pltpu.MemorySpace.HBM)] * 3
             + [pl.BlockSpec(memory_space=pltpu.VMEM)],
             scratch_shapes=[
@@ -323,26 +340,25 @@
     wide = width // steps
     whole = pl.BlockSpec(memory_space=pltpu.VMEM)
     matrix = jax.ShapeDtypeStruct((block_rows, width), jnp.bfloat16)
-    early = pl.BlockSpec((block_rows, wide), lambda i: (0, jnp.minimum(i, steps - 1)))
-    late = pl.BlockSpec((block_rows, wide), lambda i: (0, jnp.maximum(i - steps, 0)))
-    third = width // tp_count // 3
+    far = pl.BlockSpec(memory_space=pltpu.MemorySpace.HBM)
+    own_width = width // tp_count
     gate_new, up_new, down_new, partial = pl.pallas_call(
         product_kernel,
-        grid=(2 * steps,),
         out_shape=(
             matrix,
             matrix,
             matrix,
-            jax.ShapeDtypeStruct((tp_count, third, 3 * CAP), jnp.bfloat16),
+            jax.ShapeDtypeStruct((tp_count, CAP // 3, 3 * own_width), jnp.bfloat16),
         ),
         in_specs=[whole] * 2,
-        out_specs=(early, early, late, whole),
+        out_specs=(far, far, far, whole),
         scratch_shapes=[
-            pltpu.VMEM((CAP, block_rows), jnp.bfloat16),
+            pltpu.VMEM((3, block_rows, width), jnp.bfloat16),
             pltpu.VMEM((CAP, block_rows), jnp.float32),
             pltpu.VMEM((CAP, block_rows), jnp.float32),
-            pltpu.VMEM((width, CAP), jnp.float32),
+            pltpu.VMEM((CAP, width), jnp.float32),
             pltpu.VMEM((8, width), jnp.float32),
+            pltpu.SemaphoreType.DMA((3, steps)),
         ],
         compiler_params=pltpu.CompilerParams(vmem_limit_bytes=24 * 2**20),
         cost_estimate=pl.CostEstimate(

time: 124 us -> 120 us (0.968)
  Pallas kernels: 12.1 us -> 9.64 us
    pallas_call x1, Pallas kernels: 7.01 us -> 4.21 us  [shards(): pl.pallas_call(product_kernel, out_shape=(matrix, matrix, matrix, jax.Sha...]
where the time goes in v5:
time: 120 us
  blocking collectives  86.7 us (72%)
  starting transfers between devices  10.5 us (9%)
  Pallas kernels  9.64 us (8%)
  waiting for transfers between devices  9.08 us (8%)
  local copies, waits for them, and re-layouts  1.86 us (2%)
  other arithmetic  1.55 us (1%)
    all_gather x1, blocking collectives, shards(): gathered = lax.all_gather(packed.astype(jnp.float16), 'fs', axis=0)  68.4 us
    all_to_all x1, blocking collectives, shards(): lax.all_to_all(partial, 'tp', split_axis=0, concat_axis=0, tiled=True)  18.3 us
    all_to_all x1, starting transfers between devices, shards(): lax.all_to_all(pl.pallas_call(arrange_kernel, out_shape=jax.ShapeDtypeStr...  10.5 us
    all_to_all x1, waiting for transfers between devices, shards(): lax.all_to_all(pl.pallas_call(arrange_kernel, out_shape=jax.ShapeDtypeStr...  9.08 us
    pallas_call x1, Pallas kernels, shards(): pl.pallas_call(product_kernel, out_shape=(matrix, matrix, matrix, jax.Sha...  4.21 us
    pallas_call x1, Pallas kernels, shards(): pl.pallas_call(arrange_kernel, out_shape=jax.ShapeDtypeStruct((tp_count,...  2.96 us
  transfers between devices with their start and end apart: 1, of which 1 were waited for; matrix products, arithmetic and copies ran while one was open for 0% of the time, Pallas kernels for 0%

profile of v5, /device:TPU:1, one launch (start us, length us, event | category | flops | bytes accessed | tf_op | source)
XLA Modules:
  0.0 120.1 jit_solution(11526695446525791769)
XLA Ops:
  0.6 3.0 %shard_map.102 = bf16[32,48,128]{2,1,0:T(8,128)(2,1)} custom-call(f32[8,72,96]{2,1,0:T(8,128)} %bitcast.17, f32[8,72,96]{2,1,0:T(8,128)} %bitcast.18, f32[8,72,96]{2,1,0:T(8,128)} %bitcast.19, f32[1,96]{1,0:T(1,128)} %bitcast.21), custom_call_target="tpu_custom_call" | custom-call | tf_op jit(solution)/shard_map/pallas_call | solution.py:284
  3.6 10.5 %all-to-all-start = ((bf16[32,48,128]{2,1,0:T(8,128)(2,1)}), bf16[32,48,128]{2,1,0:T(8,128)(2,1)S(1)}, u32[]{:S(2)}, u32[]{:S(2)}) async-start(bf16[32,48,128]{2,1,0:T(8,128)(2,1)} %shard_map.102), calls=%async_computation | async-start | bytes 786432 | tf_op jit(solution)/shard_map/all_to_all | solution.py:283
  14.1 0.0 copy-start
  14.1 0.7 copy-done
  14.8 0.0 copy-start.3
  14.8 1.2 copy-done.3
  16.0 0.5 shard_map.104.chosen_ref
  16.5 9.1 %all-to-all-done.moved_ref = bf16[32,48,128]{2,1,0:T(8,128)(2,1)S(1)} async-done(((bf16[32,48,128]{2,1,0:T(8,128)(2,1)}), bf16[32,48,128]{2,1,0:T(8,128)(2,1)S(1)}, u32[]{:S(2)}, u32[]{:S(2)}) %all-to-all-start) | async-done | bytes 393248 | tf_op jit(solution)/shard_map/all_to_all | solution.py:283
  25.6 0.6 shard_map.103
  26.2 0.1 convert_element_type.6
  26.3 68.4 %all-gather.2 = f16[10560,384]{1,0:T(8,128)(2,1)S(1)} all-gather(f16[440,384]{1,0:T(8,128)(2,1)S(1)} %convert_element_type.6), channel_id=2, replica_groups=mesh['fs'=24,'tp'=32] {'fs'}, dimensions={0}, use_global_device_ids=true | all-gather | bytes 8448000 | tf_op jit(solution)/shard_map/all_gather | solution.py:337
  94.7 1.5 %convert_element_type.8 = bf16[10560,384]{1,0:T(8,128)(2,1)S(1)} convert(f16[10560,384]{1,0:T(8,128)(2,1)S(1)} %all-gather.2) | non-fusion elementwise | flops 4055040 | bytes 16220160 | tf_op jit(solution)/shard_map/convert_element_type | solution.py:338
  96.2 0.0 copy-start.1
  96.2 0.0 copy-start.2
  96.2 4.2 %shard_map.105 = (bf16[576,2304]{1,0:T(8,128)(2,1)}, bf16[576,2304]{1,0:T(8,128)(2,1)}, bf16[576,2304]{1,0:T(8,128)(2,1)}, bf16[32,24,216]{2,1,0:T(8,128)(2,1)S(1)}) custom-call(bf16[24,440,384]{2,1,0:T(8,128)(2,1)S(1)} %bitcast.13, bf16[72,2304]{1,0:T(8,128)(2,1)S(1)} %shard_map.104.chosen_ref), custom_call_target="tpu_custom_call" | custom-call | flops 573308928 | bytes 8388608 | tf_op jit(solution)/shard_map/pallas_call | solution.py:345
  100.4 18.3 %all_to_all.10.received_ref = bf16[32,24,216]{2,1,0:T(8,128)(2,1)S(1)} all-to-all(bf16[32,24,216]{2,1,0:T(8,128)(2,1)S(1)} %get-tuple-element.11), channel_id=1, replica_groups=mesh['fs'=24,'tp'=32] {'tp'}, dimensions={0} | all-to-all | bytes 663552 | tf_op jit(solution)/shard_map/all_to_all | solution.py:368
  118.7 0.0 copy-done.1
  118.7 0.0 copy-done.2
  118.7 1.4 %shard_map.106 = bf16[72,192]{1,0:T(8,128)(2,1)} custom-call(bf16[32,24,216]{2,1,0:T(8,128)(2,1)S(1)} %all_to_all.10.received_ref, s32[2,192]{1,0:T(2,128)S(1)} %bitcast.15, f32[2,192]{1,0:T(2,128)S(1)} %bitcast.16), custom_call_target="tpu_custom_call" | custom-call | tf_op jit(solution)/shard_map/pallas_call | solution.py:369
Async XLA Ops:
  3.6 22.0 %all-to-all-start = ((bf16[32,48,128]{2,1,0:T(8,128)(2,1)}), bf16[32,48,128]{2,1,0:T(8,128)(2,1)S(1)}, u32[]{:S(2)}, u32[]{:S(2)}) async-start(bf16[32,48,128]{2,1,0:T(8,128)(2,1)} %shard_map.102), calls=%async_computation | async-start | bytes 786432 | tf_op jit(solution)/shard_map/all_to_all | solution.py:283
  14.1 0.7 copy-start
  14.8 1.2 copy-start.3
  96.2 22.6 %copy-start.1 = (s32[192,2]{0,1:T(2,128)S(1)}, s32[192,2]{0,1:T(2,128)}, u32[]{:S(2)}) copy-start(s32[192,2]{0,1:T(2,128)} %param.12) | copy-start | bytes 4612
  96.2 22.5 %copy-start.2 = (f32[192,2]{0,1:T(2,128)S(1)}, f32[192,2]{0,1:T(2,128)}, u32[]{:S(2)}) copy-start(f32[192,2]{0,1:T(2,128)} %param.13) | copy-start | bytes 4612

commit v6 on v5

--- a/solution.py
+++ b/solution.py
@@ -15,11 +15,11 @@
     _, experts, units, _ = held.shape
     slices = out_ref.shape[0] // experts
     part = units // slices
-    half = experts // 2
+    few = experts // 4
     copies = []
-    for h in range(2):
+    for h in range(4):
         for m, source in enumerate((gate_hbm, up_hbm, down_hbm)):
-            chosen = pl.ds(h * half, half)
+            chosen = pl.ds(h * few, few)
             copy = pltpu.make_async_copy(
                 source.at[chosen], held.at[m, chosen], arrived.at[h, m]
             )
@@ -30,8 +30,8 @@
     rest = 128 - features
     gap = jnp.zeros((2, rest), jnp.float32)
     for e in range(experts):
-        if e % half == 0:
-            for copy in copies[3 * (e // half) : 3 * (e // half) + 3]:
+        if e % few == 0:
+            for copy in copies[3 * (e // few) : 3 * (e // few) + 3]:
                 copy.wait()
         for s in range(slices):
             rows = slice(s * part, (s + 1) * part)
@@ -288,7 +288,7 @@
             + [pl.BlockSpec(memory_space=pltpu.VMEM)],
             scratch_shapes=[
                 pltpu.VMEM((3, experts, slices * units, features), jnp.float32),
-                pltpu.SemaphoreType.DMA((2, 3)),
+                pltpu.SemaphoreType.DMA((4, 3)),
             ],
             compiler_params=pltpu.CompilerParams(vmem_limit_bytes=60 * 1024 * 2**10),
         )(

time: 120 us -> 121 us (level)
  no operation moved by 1% of the time
where the time goes in v6:
time: 121 us; the launch traced here: 120 us
  blocking collectives  86.7 us (72%)
  starting transfers between devices  10.5 us (9%)
  Pallas kernels  9.79 us (8%)
  waiting for transfers between devices  9.08 us (8%)
  local copies, waits for them, and re-layouts  1.86 us (2%)
  other arithmetic  1.55 us (1%)
    all_gather x1, blocking collectives, shards(): gathered = lax.all_gather(packed.astype(jnp.float16), 'fs', axis=0)  68.4 us
    all_to_all x1, blocking collectives, shards(): lax.all_to_all(partial, 'tp', split_axis=0, concat_axis=0, tiled=True)  18.3 us
    all_to_all x1, starting transfers between devices, shards(): lax.all_to_all(pl.pallas_call(arrange_kernel, out_shape=jax.ShapeDtypeStr...  10.5 us
    all_to_all x1, waiting for transfers between devices, shards(): lax.all_to_all(pl.pallas_call(arrange_kernel, out_shape=jax.ShapeDtypeStr...  9.08 us
    pallas_call x1, Pallas kernels, shards(): pl.pallas_call(product_kernel, out_shape=(matrix, matrix, matrix, jax.Sha...  4.22 us
    pallas_call x1, Pallas kernels, shards(): pl.pallas_call(arrange_kernel, out_shape=jax.ShapeDtypeStruct((tp_count,...  3.1 us
  transfers between devices with their start and end apart: 1, of which 1 were waited for; matrix products, arithmetic and copies ran while one was open for 0% of the time, Pallas kernels for 0%

profile of v6, /device:TPU:1, one launch (start us, length us, event | category | flops | bytes accessed | tf_op | source)
XLA Modules:
  0.0 120.2 jit_solution(5238278801916587386)
XLA Ops:
  0.6 3.1 %shard_map.102 = bf16[32,48,128]{2,1,0:T(8,128)(2,1)} custom-call(f32[8,72,96]{2,1,0:T(8,128)} %bitcast.17, f32[8,72,96]{2,1,0:T(8,128)} %bitcast.18, f32[8,72,96]{2,1,0:T(8,128)} %bitcast.19, f32[1,96]{1,0:T(1,128)} %bitcast.21), custom_call_target="tpu_custom_call" | custom-call | tf_op jit(solution)/shard_map/pallas_call | solution.py:284
  3.7 10.5 %all-to-all-start = ((bf16[32,48,128]{2,1,0:T(8,128)(2,1)}), bf16[32,48,128]{2,1,0:T(8,128)(2,1)S(1)}, u32[]{:S(2)}, u32[]{:S(2)}) async-start(bf16[32,48,128]{2,1,0:T(8,128)(2,1)} %shard_map.102), calls=%async_computation | async-start | bytes 786432 | tf_op jit(solution)/shard_map/all_to_all | solution.py:283
  14.3 0.0 copy-start
  14.3 0.7 copy-done
  15.0 0.0 copy-start.3
  15.0 1.2 copy-done.3
  16.1 0.5 shard_map.104.chosen_ref
  16.7 9.1 %all-to-all-done.moved_ref = bf16[32,48,128]{2,1,0:T(8,128)(2,1)S(1)} async-done(((bf16[32,48,128]{2,1,0:T(8,128)(2,1)}), bf16[32,48,128]{2,1,0:T(8,128)(2,1)S(1)}, u32[]{:S(2)}, u32[]{:S(2)}) %all-to-all-start) | async-done | bytes 393248 | tf_op jit(solution)/shard_map/all_to_all | solution.py:283
  25.8 0.6 shard_map.103
  26.3 0.1 convert_element_type.6
  26.4 68.4 %all-gather.2 = f16[10560,384]{1,0:T(8,128)(2,1)S(1)} all-gather(f16[440,384]{1,0:T(8,128)(2,1)S(1)} %convert_element_type.6), channel_id=2, replica_groups=mesh['fs'=24,'tp'=32] {'fs'}, dimensions={0}, use_global_device_ids=true | all-gather | bytes 8448000 | tf_op jit(solution)/shard_map/all_gather | solution.py:337
  94.8 1.5 %convert_element_type.8 = bf16[10560,384]{1,0:T(8,128)(2,1)S(1)} convert(f16[10560,384]{1,0:T(8,128)(2,1)S(1)} %all-gather.2) | non-fusion elementwise | flops 4055040 | bytes 16220160 | tf_op jit(solution)/shard_map/convert_element_type | solution.py:338
  96.3 0.0 copy-start.1
  96.3 0.0 copy-start.2
  96.3 4.2 %shard_map.105 = (bf16[576,2304]{1,0:T(8,128)(2,1)}, bf16[576,2304]{1,0:T(8,128)(2,1)}, bf16[576,2304]{1,0:T(8,128)(2,1)}, bf16[32,24,216]{2,1,0:T(8,128)(2,1)S(1)}) custom-call(bf16[24,440,384]{2,1,0:T(8,128)(2,1)S(1)} %bitcast.13, bf16[72,2304]{1,0:T(8,128)(2,1)S(1)} %shard_map.104.chosen_ref), custom_call_target="tpu_custom_call" | custom-call | flops 573308928 | bytes 8388608 | tf_op jit(solution)/shard_map/pallas_call | solution.py:345
  100.6 18.3 %all_to_all.10.received_ref = bf16[32,24,216]{2,1,0:T(8,128)(2,1)S(1)} all-to-all(bf16[32,24,216]{2,1,0:T(8,128)(2,1)S(1)} %get-tuple-element.11), channel_id=1, replica_groups=mesh['fs'=24,'tp'=32] {'tp'}, dimensions={0} | all-to-all | bytes 663552 | tf_op jit(solution)/shard_map/all_to_all | solution.py:368
  118.9 0.0 copy-done.1
  118.9 0.0 copy-done.2
  118.9 1.4 %shard_map.106 = bf16[72,192]{1,0:T(8,128)(2,1)} custom-call(bf16[32,24,216]{2,1,0:T(8,128)(2,1)S(1)} %all_to_all.10.received_ref, s32[2,192]{1,0:T(2,128)S(1)} %bitcast.15, f32[2,192]{1,0:T(2,128)S(1)} %bitcast.16), custom_call_target="tpu_custom_call" | custom-call | tf_op jit(solution)/shard_map/pallas_call | solution.py:369
Async XLA Ops:
  3.7 22.0 %all-to-all-start = ((bf16[32,48,128]{2,1,0:T(8,128)(2,1)}), bf16[32,48,128]{2,1,0:T(8,128)(2,1)S(1)}, u32[]{:S(2)}, u32[]{:S(2)}) async-start(bf16[32,48,128]{2,1,0:T(8,128)(2,1)} %shard_map.102), calls=%async_computation | async-start | bytes 786432 | tf_op jit(solution)/shard_map/all_to_all | solution.py:283
  14.3 0.7 copy-start
  15.0 1.2 copy-start.3
  96.3 22.6 %copy-start.1 = (s32[192,2]{0,1:T(2,128)S(1)}, s32[192,2]{0,1:T(2,128)}, u32[]{:S(2)}) copy-start(s32[192,2]{0,1:T(2,128)} %param.12) | copy-start | bytes 4612
  96.3 22.5 %copy-start.2 = (f32[192,2]{0,1:T(2,128)S(1)}, f32[192,2]{0,1:T(2,128)}, u32[]{:S(2)}) copy-start(f32[192,2]{0,1:T(2,128)} %param.13) | copy-start | bytes 4612
